TPU v7x, 256 devices: a whole 4x4x8 slice. The times are simulated.
256 devices in a mesh: sp: 32 (over z, y), fs: 4 (over x), tp: 2 (over core).
Axes of the slice: x: 4, y: 4, z: 8, core: 2. Of those that a mesh axis runs over, the one named last changes fastest.
Arguments:
- tokens: bfloat16 [16384, 2048], P(('fs', 'sp'), 'tp'), parts along dimension 0, may hold values from -6 to 6
- norm_gain: float32 [2048], replicated, may hold values from 0.1 to 1.9
- w_recur_in: bfloat16 [2048, 1024], P(None, 'tp'), may hold values from -0.125 to 0.125
- conv_weight: float32 [4, 1024], P(None, 'tp'), may hold values from -3 to 3
- w_gate_decay: bfloat16 [16, 64, 64], P('tp'), may hold values from -0.75 to 0.75
- w_gate_input: bfloat16 [16, 64, 64], P('tp'), may hold values from -0.75 to 0.75
- decay_base: float32 [1024], P('tp'), may hold values from 0 to 0.01, as said below
- extra_decay: float32 [16384, 16], P(('fs', 'sp'), 'tp'), parts along dimension 0, may hold values from 0 to 1, as said below
- w_query: bfloat16 [2048, 1024], P(None, 'tp'), may hold values from -1 to 1
- w_key: bfloat16 [2048, 256], P(None, 'tp'), may hold values from -20 to 20
- w_value: bfloat16 [2048, 256], P(None, 'tp'), may hold values from -0.125 to 0.125
- mix_lambda: float32 [8], P('tp'), may hold values from 0.3 to 0.8
- head_gain: float32 [128], replicated, may hold values from 0.1 to 1.9
- w_out_recur: bfloat16 [1024, 2048], P('tp'), may hold values from -0.125 to 0.125
- w_out_attend: bfloat16 [1024, 2048], P('tp'), may hold values from -0.125 to 0.125
- out_gain: float32 [2048], replicated, may hold values from 0.1 to 1.9
Outputs:
- mixed: bfloat16 [16384, 2048], P(('fs', 'sp', 'tp')), parts along dimension 0
There are 4 independent parts, one for each index of `fs`. A program takes and returns all parts, laid end to end along the dimension named above; an argument that names none is the same for every part. Nothing has to cross between parts.
Inputs may be any that keep to these rules, and one draw needn't show every extreme that they name: `decay_base`: positive rates of each channel. `extra_decay`: non-negative added log-decays.
All inputs are finite; a program needn't handle non-finite values.
Results may differ from a plain program's by a relative error of at most 0.012.
The roundings to bfloat16 on the way count: a program that leaves them out, or rounds other values in their place, can miss the bound.
Values may be sent and summed in bfloat16 or wider, within the bound.
No kernel may reach another device: no remote copies, remote signals or barrier semaphores. Data moves between devices by JAX's collectives and lax.ppermute only.
A program may use at most 128 MiB of HBM per device.

v0:
```python
import functools

import jax
import jax.numpy as jnp
from jax import lax
from jax.experimental import pallas as pl
from jax.experimental.pallas import tpu as pltpu
from jax.sharding import PartitionSpec as P


D = 2048
HEAD = 64
DV = 128
NY = 4
NZ = 8
lru_rate = 8.0
norm_eps = 1e-06
COLS = 128
EXTRA = 16
f32 = jnp.float32
bf16 = jnp.bfloat16


def sp_pairs(dz, dy):
    return [
        (z * NY + y, (z + dz) % NZ * NY + (y + dy) % NY) for z in range(NZ) for y in range(NY)
    ]


def around():
    return [
        (2 * i + t, 2 * ((z + 1 - 2 * t) % NZ * NY + y) + t)
        for i in range(NZ * NY)
        for z, y in [divmod(i, NY)]
        for t in range(2)
    ]


def later(flip):
    return [(2 * i + t, 2 * i + 2 + (t ^ flip)) for i in range(NZ * NY - 1) for t in range(2)]


def attend_block(kv, q_ref, acc_ref, stat_ref, score_ref, expo_ref, mask=None):
    keys = kv[:, : 2 * HEAD]
    values_t = kv[:, 2 * HEAD :].T
    cols = score_ref.shape[2]
    steps = q_ref.shape[0] // cols

    def score(i):
        score_ref[i % 2] = lax.dot_general(
            keys,
            q_ref[i * cols : (i + 1) * cols, :],
            (((1,), (1,)), ((), ())),
            preferred_element_type=f32,
        )

    def soften(i):
        part = slice(i * cols, (i + 1) * cols)
        scores = score_ref[i % 2]
        if mask is not None:
            scores = jnp.where(mask, scores, -1e30)
        old = stat_ref[0:1, part]
        peak = jnp.maximum(old, jnp.max(scores, axis=0, keepdims=True))
        fix = jnp.exp(old - peak)
        expo = jnp.exp(scores - peak)
        stat_ref[0:1, part] = peak
        stat_ref[1:2, part] = stat_ref[1:2, part] * fix + jnp.sum(expo, axis=0, keepdims=True)
        expo_ref[i % 2] = expo.astype(bf16)
        acc_ref[:, part] = acc_ref[:, part] * fix

    def gain(i):
        part = slice(i * cols, (i + 1) * cols)
        acc_ref[:, part] += jnp.dot(values_t, expo_ref[i % 2], preferred_element_type=f32)

    score(0)
    for i in range(steps):
        if i + 1 < steps:
            score(i + 1)
        soften(i)
        if i > 0:
            gain(i - 1)
    gain(steps - 1)


def attend_scratch(keys):
    return [pltpu.VMEM((2, keys, COLS), f32), pltpu.VMEM((2, keys, COLS), bf16)]


def first_kernel(
    wide_ref,
    block_ref,
    acc_ref,
    stat_ref,
    score_ref,
    expo_ref,
):
    rows = wide_ref.shape[0] // 8
    acc_ref[...] = jnp.zeros_like(acc_ref)
    stat_ref[...] = jnp.zeros_like(stat_ref)
    stat_ref[0:1, :] = jnp.full((1, stat_ref.shape[1]), -1e30, f32)
    count, cols = NY * rows, COLS
    key_at = lax.broadcasted_iota(jnp.int32, (count, cols), 0)
    query_at = lax.broadcasted_iota(jnp.int32, (count, cols), 1) % rows
    own_y = lax.axis_index("sp") % NY
    mask = key_at <= jnp.where(key_at < rows, query_at, own_y * rows + rows - 1)
    attend_block(block_ref[EXTRA:, :], wide_ref, acc_ref, stat_ref, score_ref, expo_ref, mask)


def take_block(step, up, parts, wide_ref, acc_ref, stat_ref, carry_ref, score_ref, expo_ref):
    own_z = lax.axis_index("sp") // NY
    needed = jnp.where(up, own_z, own_z + 2 * step - NZ) >= step

    @pl.when(needed)
    def _():
        block = jnp.concatenate([parts[0][EXTRA:, :]] + [part[...] for part in parts[1:]], axis=0)
        attend_block(block, wide_ref, acc_ref, stat_ref, score_ref, expo_ref)

    @pl.when(jnp.logical_and(needed, up))
    def _():
        decay, state = unpacked(parts[0][:EXTRA, :])
        before = carry_ref[0:1, :]
        carry_ref[1:2, :] = before * state + carry_ref[1:2, :]
        carry_ref[0:1, :] = before * decay

    @pl.when(jnp.logical_and(needed, jnp.logical_not(up)))
    def _():
        decay, state = unpacked(parts[0][:EXTRA, :])
        carry_ref[3:4, :] = decay * carry_ref[3:4, :] + state
        carry_ref[2:3, :] = decay * carry_ref[2:3, :]


def more_kernel(wide_ref, *refs, steps):
    n = sum(count for _, _, count in steps)
    blocks, (acc_in, stat_in, carry_in) = list(refs[:n]), refs[n : n + 3]
    acc_ref, stat_ref, carry_ref, score_ref, expo_ref = refs[n + 3 :]
    acc_ref[...] = acc_in[...]
    stat_ref[...] = stat_in[...]
    carry_ref[...] = carry_in[...]
    core = lax.axis_index("tp")
    refs = (wide_ref, acc_ref, stat_ref, carry_ref, score_ref, expo_ref)
    for step, up_core, count in steps:
        parts, blocks = blocks[:count], blocks[count:]
        take_block(step, core == up_core, parts, *refs)


SMEM = pl.BlockSpec(memory_space=pltpu.SMEM)
PARAMS = pltpu.CompilerParams(vmem_limit_bytes=16 << 20)
VMEM = pl.BlockSpec(memory_space=pltpu.VMEM)
ANY = pl.BlockSpec(memory_space=pltpu.HBM)


def attend_first(wide, block):
    return pl.pallas_call(
        first_kernel,
        out_shape=(
            jax.ShapeDtypeStruct((DV, wide.shape[0]), f32),
            jax.ShapeDtypeStruct((8, wide.shape[0]), f32),
        ),
        in_specs=[VMEM] * 2,
        out_specs=(VMEM,) * 2,
        scratch_shapes=attend_scratch(block.shape[0] - EXTRA),
        compiler_params=PARAMS,
        name="attend_first",
        cost_estimate=pl.CostEstimate(flops=4 << 30, bytes_accessed=1 << 20, transcendentals=0),
    )(wide, block)


def attend_more(wide, waiting, state):
    blocks = [part for parts, _, _ in waiting for part in parts]
    steps = tuple((step, up_core, len(parts)) for parts, step, up_core in waiting)
    n = len(blocks)
    return pl.pallas_call(
        functools.partial(more_kernel, steps=steps),
        out_shape=tuple(jax.ShapeDtypeStruct(a.shape, f32) for a in state),
        in_specs=[VMEM] * (n + 4),
        out_specs=(VMEM,) * 3,
        input_output_aliases={n + 1: 0, n + 2: 1, n + 3: 2},
        scratch_shapes=attend_scratch(sum(part.shape[0] for part in waiting[0][0]) - EXTRA),
        compiler_params=PARAMS,
        name="attend_more",
        cost_estimate=pl.CostEstimate(flops=4 << 30, bytes_accessed=1 << 20, transcendentals=0),
    )(wide, *blocks, *state)


def last_kernel(
    lambda_ref,
    gain_ref,
    wide_ref,
    one_ref,
    two_ref,
    acc_in,
    stat_in,
    carry_in,
    cum_ref,
    local_ref,
    recur_w_ref,
    attend_w_ref,
    keep_ref,
    send_ref,
    acc_ref,
    stat_ref,
    carry_ref,
    score_ref,
    expo_ref,
    *,
    step,
):
    acc_ref[...] = acc_in[...]
    stat_ref[...] = stat_in[...]
    carry_ref[...] = carry_in[...]
    refs = (wide_ref, acc_ref, stat_ref, carry_ref, score_ref, expo_ref)
    take_block(step, lax.axis_index("tp") >= 0, (one_ref, two_ref), *refs)
    before = carry_ref[0:1, :] * carry_ref[3:4, :] + carry_ref[1:2, :]
    recur_out = (local_ref[...] + cum_ref[...] * before).astype(bf16)
    rows = recur_out.shape[0]
    heads = acc_ref.shape[1] // (2 * rows)
    inverse = 1.0 / stat_ref[1:2, :]
    attend_out = []
    for head in range(heads):
        one = slice(head * rows, (head + 1) * rows)
        two = slice((heads + head) * rows, (heads + head + 1) * rows)
        out = acc_ref[:, one] * inverse[:, one] - lambda_ref[head] * (
            acc_ref[:, two] * inverse[:, two]
        )
        mean = jnp.mean(out * out, axis=0, keepdims=True)
        attend_out.append(((out * lax.rsqrt(mean + norm_eps)).T * gain_ref[...]).astype(bf16))
    total = jnp.dot(recur_out, recur_w_ref[...], preferred_element_type=f32) + jnp.dot(
        jnp.concatenate(attend_out, axis=1), attend_w_ref[...], preferred_element_type=f32
    )
    keep_low = lax.axis_index("tp") == 0
    half = rows // 2
    keep_ref[...] = jnp.where(keep_low, total[:half], total[half:])
    send_ref[...] = jnp.where(keep_low, total[half:], total[:half]).astype(bf16)


def last_part(lambdas, gain, wide, halves, step, state, cum, local, recur_w, attend_w):
    rows, cols = cum.shape[0], recur_w.shape[1]
    return pl.pallas_call(
        functools.partial(last_kernel, step=step),
        out_shape=(
            jax.ShapeDtypeStruct((rows // 2, cols), f32),
            jax.ShapeDtypeStruct((rows // 2, cols), bf16),
        ),
        in_specs=[SMEM] + [VMEM] * 11,
        out_specs=(VMEM, VMEM),
        scratch_shapes=[pltpu.VMEM(a.shape, f32) for a in state]
        + attend_scratch(2 * halves[1].shape[0]),
        compiler_params=PARAMS,
        name="last_part",
        cost_estimate=pl.CostEstimate(flops=4 << 30, bytes_accessed=4 << 20, transcendentals=0),
    )(lambdas, gain, wide, *halves, *state, cum, local, recur_w, attend_w)


def norm_kernel(keep_ref, got_ref, gain_ref, out_ref):
    merged = keep_ref[...] + got_ref[...].astype(f32)
    mean = jnp.mean(merged * merged, axis=1, keepdims=True)
    out_ref[...] = (merged * lax.rsqrt(mean + norm_eps) * gain_ref[...]).astype(bf16)


def final_norm(keep, got, gain):
    return pl.pallas_call(
        norm_kernel,
        out_shape=jax.ShapeDtypeStruct(keep.shape, bf16),
        in_specs=[VMEM] * 3,
        out_specs=VMEM,
        compiler_params=PARAMS,
        name="final_norm",
    )(keep, got, gain)


def negative_expm1(y):
    series = 1.0 + y * (1.0 / 8.0)
    for k in (7, 6, 5, 4, 3, 2):
        series = 1.0 + y * (1.0 / k) * series
    return jnp.where(y > -0.5, -y * series, 1.0 - jnp.exp(y))


def packed(value):
    rows = []
    for _ in range(3):
        term = value.astype(bf16).astype(f32)
        value = value - term
        rows += [term[:, :256], term[:, 256:]]
    return rows


def unpacked(rows):
    rows = rows.astype(f32)
    sums = []
    for at in (0, 6):
        halves = [
            rows[at + half : at + half + 1]
            + rows[at + half + 2 : at + half + 3]
            + rows[at + half + 4 : at + half + 5]
            for half in range(2)
        ]
        sums.append(jnp.concatenate(halves, axis=1))
    return sums


def written(decay, state):
    rows = packed(decay) + packed(state)
    rows += [jnp.zeros_like(rows[0])] * (EXTRA - len(rows))
    return jnp.concatenate(rows, axis=0).astype(bf16)


def in_hbm(*arrays):
    return [pltpu.with_memory_space_constraint(a, pltpu.HBM) for a in arrays]


def started(pairs, sems):
    copies = [pltpu.make_async_copy(src, dst, sems.at[i]) for i, (src, dst) in enumerate(pairs)]
    for copy in copies:
        copy.start()
    return copies


def own_kernel(
    tokens_ref, gain_ref, *refs
):
    weights, (acc_ref, square_ref, own_ref, other_ref, held_ref, gain_held, sems) = refs[:4], refs[4:]
    width = tokens_ref.shape[1]
    tp = lax.axis_index("tp")
    mine = pl.ds(pl.multiple_of(tp * width, width), width)
    theirs = pl.ds(pl.multiple_of((1 - tp) * width, width), width)
    pairs = [(tokens_ref, held_ref), (gain_ref, gain_held)]
    parts, at = [], 0
    for w_ref in weights:
        parts.append(slice(at, at + w_ref.shape[1]))
        at += w_ref.shape[1]
    pairs += [(w_ref.at[mine, :], own_ref.at[:, part]) for w_ref, part in zip(weights, parts)]
    pairs += [(w_ref.at[theirs, :], other_ref.at[:, part]) for w_ref, part in zip(weights, parts)]
    copies = started(pairs, sems)
    copies[0].wait()
    copies[1].wait()
    tokens = held_ref[...].astype(f32)
    scaled = (tokens * gain_held[:, mine]).astype(bf16)
    square_ref[...] = jnp.broadcast_to(
        jnp.sum(tokens * tokens, axis=1, keepdims=True), square_ref.shape
    )
    for copy, part in zip(copies[2:6], parts):
        copy.wait()
        acc_ref[:, part] = jnp.dot(scaled, own_ref[:, part], preferred_element_type=f32)
    for copy in copies[6:]:
        copy.wait()


def project_own(tokens, gain, *weights):
    rows, width = tokens.shape
    cols = sum(w.shape[1] for w in weights)
    half = jax.ShapeDtypeStruct((width, cols), bf16)
    return pl.pallas_call(
        own_kernel,
        out_shape=(
            jax.ShapeDtypeStruct((rows, cols), f32),
            jax.ShapeDtypeStruct((rows, 128), f32),
            half,
            half,
        ),
        in_specs=[ANY] * 6,
        out_specs=(VMEM,) * 4,
        scratch_shapes=[
            pltpu.VMEM(tokens.shape, bf16),
            pltpu.VMEM(gain.shape, f32),
            pltpu.SemaphoreType.DMA((10,)),
        ],
        compiler_params=PARAMS,
        name="project_own",
        cost_estimate=pl.CostEstimate(flops=2 << 30, bytes_accessed=4 << 20, transcendentals=0),
    )(*in_hbm(tokens, gain, *weights))


def front_kernel(
    acc_ref,
    square_ref,
    own_w_ref,
    other_w_ref,
    other_ref,
    halo_own_ref,
    halo_other_ref,
    gain_hbm,
    taps_hbm,
    decay_hbm,
    input_hbm,
    base_hbm,
    extra_hbm,
    out_recur_hbm,
    out_attend_hbm,
    piece_ref,
    wide_ref,
    cum_ref,
    state_ref,
    out_recur_ref,
    out_attend_ref,
    padded_ref,
    gain_ref,
    taps_ref,
    decay_w_ref,
    input_w_ref,
    base_ref,
    extra_ref,
    sems,
):
    rows, width = other_ref.shape
    cols = cum_ref.shape[1]
    taps = taps_ref.shape[0]
    copies = started(
        [
            (gain_hbm, gain_ref),
            (taps_hbm, taps_ref),
            (decay_hbm, decay_w_ref),
            (input_hbm, input_w_ref),
            (base_hbm, base_ref),
            (extra_hbm, extra_ref),
            (out_recur_hbm, out_recur_ref),
            (out_attend_hbm, out_attend_ref),
        ],
        sems,
    )
    tp = lax.axis_index("tp")
    mine = pl.ds(pl.multiple_of(tp * width, width), width)
    theirs = pl.ds(pl.multiple_of((1 - tp) * width, width), width)
    copies[0].wait()

    def scaled(tokens, part):
        return (tokens * gain_ref[:, part]).astype(bf16)

    other = other_ref[...].astype(f32)
    square = square_ref[:, 0:1] + jnp.sum(other * other, axis=1, keepdims=True)
    inverse = lax.rsqrt(square / D + norm_eps)
    scaled_other = scaled(other, theirs)

    def project(at, count):
        lanes = slice(at, at + count)
        part = jnp.dot(scaled_other, other_w_ref[:, lanes], preferred_element_type=f32)
        return (acc_ref[:, lanes] + part) * inverse

    halo_own, halo_other = halo_own_ref[...].astype(f32), halo_other_ref[...].astype(f32)
    square = jnp.sum(halo_own * halo_own, axis=1, keepdims=True) + jnp.sum(
        halo_other * halo_other, axis=1, keepdims=True
    )
    halo = jnp.dot(scaled(halo_own, mine), own_w_ref[:, :cols], preferred_element_type=f32)
    both = jnp.dot(
        jnp.concatenate([scaled_other, scaled(halo_other, theirs)], axis=0),
        other_w_ref[:, :cols],
        preferred_element_type=f32,
    )
    halo = ((halo + both[rows:]) * lax.rsqrt(square / D + norm_eps)).astype(bf16)
    padded_ref[0:8, :] = halo.astype(f32)
    recur_in = ((acc_ref[:, :cols] + both[:rows]) * inverse).astype(bf16)
    padded_ref[8 : 8 + rows, :] = recur_in.astype(f32)

    at = own_w_ref.shape[1] - 2 * HEAD - DV
    piece_ref[:rows, : 2 * HEAD] = project(at, 2 * HEAD).astype(bf16)
    piece_ref[:rows, 2 * HEAD :] = project(at + 2 * HEAD, DV).astype(bf16)

    queries = project(cols, at - cols).astype(bf16) * HEAD ** (-0.5)
    heads = queries.shape[1] // (2 * HEAD)
    first = lax.broadcasted_iota(jnp.int32, (rows, 2 * HEAD), 1) < HEAD
    for head in range(heads):
        part = queries[:, head * 2 * HEAD : (head + 1) * 2 * HEAD]
        zero = jnp.zeros_like(part)
        wide_ref[head * rows : (head + 1) * rows, :] = jnp.where(first, part, zero)
        begin = (heads + head) * rows
        wide_ref[begin : begin + rows, :] = jnp.where(first, zero, part)

    for copy in copies[1:6]:
        copy.wait()
    extra_decay = extra_ref[...].T
    row = lax.broadcasted_iota(jnp.int32, (rows, 128), 0)
    low = lax.broadcasted_iota(jnp.int32, (rows, 128), 1) < HEAD
    square = lax.broadcasted_iota(jnp.int32, (128, 128), 0) < HEAD
    same = square == (lax.broadcasted_iota(jnp.int32, (128, 128), 1) < HEAD)
    totals = []
    for pair in range(cols // 128):
        lanes = slice(pair * 128, (pair + 1) * 128)
        conv = jnp.zeros((rows, 128), f32)
        for tap in range(taps):
            begin = 8 - (taps - 1) + tap
            conv = conv + taps_ref[tap : tap + 1, lanes] * padded_ref[begin : begin + rows, lanes]
        conv_in = conv.astype(bf16)

        def gate(w_ref):
            both = jnp.concatenate([w_ref[2 * pair], w_ref[2 * pair + 1]], axis=0)
            both = jnp.concatenate([both, both], axis=1)
            both = jnp.where(same, both, jnp.zeros_like(both))
            return jax.nn.sigmoid(jnp.dot(conv_in, both, preferred_element_type=f32))

        decay_gate = gate(decay_w_ref)
        input_gate = gate(input_w_ref)
        extra = jnp.where(
            low,
            extra_decay[:, 2 * pair : 2 * pair + 1],
            extra_decay[:, 2 * pair + 1 : 2 * pair + 2],
        )
        log_decay = -lru_rate * decay_gate * base_ref[:, lanes] - extra
        decay = jnp.exp(log_decay)
        inject = jnp.sqrt(negative_expm1(2.0 * log_decay)) * input_gate * conv_in.astype(f32)
        step = 1
        while step < rows:
            if step < 8:
                keep = row >= step
                decay_before = jnp.where(keep, pltpu.roll(decay, step, 0), 1.0)
                inject_before = jnp.where(keep, pltpu.roll(inject, step, 0), 0.0)
            else:
                one = jnp.ones((step, 128), f32)
                decay_before = jnp.concatenate([one, decay[:-step]], axis=0)
                inject_before = jnp.concatenate([jnp.zeros_like(one), inject[:-step]], axis=0)
            inject = inject + decay * inject_before
            decay = decay * decay_before
            step *= 2
        cum_ref[:, lanes] = decay
        state_ref[:, lanes] = inject
        totals.append((decay[rows - 1 :], inject[rows - 1 :]))
    decay, state = (jnp.concatenate(t, axis=1) for t in zip(*totals))
    piece_ref[rows:, :] = written(decay, state)
    for copy in copies[6:]:
        copy.wait()


def front(own, other, halos, small, out_weights, cols):
    rows = other.shape[0]
    queries = own[0].shape[1] - cols - 2 * HEAD - DV
    whole = jax.ShapeDtypeStruct((rows, cols), f32)
    return pl.pallas_call(
        front_kernel,
        out_shape=(
            jax.ShapeDtypeStruct((rows + EXTRA, 2 * HEAD + DV), bf16),
            jax.ShapeDtypeStruct((2 * rows * queries // (2 * HEAD), 2 * HEAD), bf16),
            whole,
            whole,
            *(jax.ShapeDtypeStruct(w.shape, bf16) for w in out_weights),
        ),
        in_specs=[VMEM] * 7 + [ANY] * 8,
        out_specs=(VMEM,) * 6,
        scratch_shapes=[pltpu.VMEM((rows + 8, cols), f32)]
        + [pltpu.VMEM(a.shape, a.dtype) for a in small]
        + [pltpu.SemaphoreType.DMA((8,))],
        compiler_params=PARAMS,
        name="front",
        cost_estimate=pl.CostEstimate(flops=4 << 30, bytes_accessed=1 << 20, transcendentals=0),
    )(*own, other, *halos, *in_hbm(*small, *out_weights))


def assemble_kernel(*refs):
    pieces, (block_ref, one_ref, two_ref, carry_ref, each_ref) = refs[:NY], refs[NY:]
    rows = pieces[0].shape[0] - EXTRA
    for r, piece in enumerate(pieces):
        begin = EXTRA + r * rows
        block_ref[begin : begin + rows, :] = piece[:rows, :]
        half_ref, begin = (one_ref, begin) if r < NY // 2 else (two_ref, (r - NY // 2) * rows)
        half_ref[begin : begin + rows, :] = piece[:rows, :]
        decay, state = unpacked(piece[rows:, :])
        each_ref[r, 0:1, :] = decay
        each_ref[r, 1:2, :] = state
    own_y = lax.axis_index("sp") % NY
    decay, state = each_ref[own_y, 0:1, :], each_ref[own_y, 1:2, :]
    before = [jnp.ones_like(decay), jnp.zeros_like(state)]
    for y in range(1, NY):
        earlier = y - 1 < own_y
        before = [
            jnp.where(earlier, decay, before[0]),
            jnp.where(earlier, state, before[1]),
        ]
        earlier = y <= own_y
        at = lax.rem(own_y - y + NY, NY)
        this = each_ref[at, 0:1, :]
        state = this * state + each_ref[at, 1:2, :]
        decay = this * decay
    block_ref[:EXTRA, :] = one_ref[:EXTRA, :] = written(decay, state)
    carry_ref[...] = jnp.zeros_like(carry_ref)
    carry_ref[0:1, :] = before[0]
    carry_ref[1:2, :] = before[1]
    carry_ref[2:3, :] = jnp.ones_like(decay)


def assemble(pieces, cols):
    rows, width = pieces[0].shape
    return pl.pallas_call(
        assemble_kernel,
        out_shape=(
            jax.ShapeDtypeStruct((NY * (rows - EXTRA) + EXTRA, width), bf16),
            jax.ShapeDtypeStruct((NY // 2 * (rows - EXTRA) + EXTRA, width), bf16),
            jax.ShapeDtypeStruct((NY // 2 * (rows - EXTRA), width), bf16),
            jax.ShapeDtypeStruct((8, cols), f32),
        ),
        in_specs=[VMEM] * NY,
        out_specs=(VMEM,) * 4,
        scratch_shapes=[pltpu.VMEM((NY, 8, cols), f32)],
        compiler_params=PARAMS,
        name="assemble",
    )(*pieces)


def layer(
    tokens,
    norm_gain,
    w_recur_in,
    conv_weight,
    w_gate_decay,
    w_gate_input,
    decay_base,
    extra_decay,
    w_query,
    w_key,
    w_value,
    mix_lambda,
    head_gain,
    w_out_recur,
    w_out_attend,
    out_gain,
):
    rows = tokens.shape[0]
    recur_cols = w_recur_in.shape[1]
    weights = (w_recur_in, w_query, w_key, w_value)
    gain = norm_gain[None, :]

    swap = [(0, 1), (1, 0)]
    other = lax.ppermute(tokens, "tp", swap)
    ends = tokens[rows - 8 :]
    halo_own = lax.ppermute(ends, ("sp", "tp"), later(0))
    halo_other = lax.ppermute(ends, ("sp", "tp"), later(1))
    own = project_own(tokens, gain, *weights)
    small = (gain, conv_weight, w_gate_decay, w_gate_input, decay_base[None, :], extra_decay.T)
    piece, wide, cum, local, w_out_recur, w_out_attend = front(
        own, other, (halo_own, halo_other), small, (w_out_recur, w_out_attend), recur_cols
    )

    pieces = [piece] + [lax.ppermute(piece, "sp", sp_pairs(0, r)) for r in range(1, NY)]
    block, *same, carry = assemble(pieces, recur_cols)

    state = (*attend_first(wide, block), carry)
    cross = lax.ppermute(block, "tp", swap)
    waiting = []
    for step in range(1, NZ // 2 + 1):
        for i in range(2):
            same[i] = lax.ppermute(same[i], ("sp", "tp"), around())
        if step == NZ // 2:
            break
        waiting.append((tuple(same), step, 0))
        state = attend_more(wide, waiting, state)
        cross = lax.ppermute(cross, ("sp", "tp"), around())
        other = lax.ppermute(cross, "tp", swap)
        waiting = [((other,), step, 1)]
    state = attend_more(wide, waiting, state)
    keep, send = last_part(
        mix_lambda,
        head_gain[None, :],
        wide,
        same,
        NZ // 2,
        state,
        cum,
        local,
        w_out_recur,
        w_out_attend,
    )
    got = lax.ppermute(send, "tp", swap)
    return final_norm(keep, got, out_gain[None, :])


def solution(mesh):
    in_specs = (
        P(("fs", "sp"), "tp"),
        P(),
        P(None, "tp"),
        P(None, "tp"),
        P("tp", None, None),
        P("tp", None, None),
        P("tp"),
        P(("fs", "sp"), "tp"),
        P(None, "tp"),
        P(None, "tp"),
        P(None, "tp"),
        P("tp"),
        P(),
        P("tp", None),
        P("tp", None),
        P(),
    )
    out_specs = P(("fs", "sp", "tp"), None)
    return jax.shard_map(layer, mesh=mesh, in_specs=in_specs, out_specs=out_specs, check_vma=False)
```

profile of v0, /device:TPU:1, one launch (start us, length us, event | category | flops | bytes accessed | tf_op | source)
XLA Modules:
  0.0 66.1 jit_solution(14327165399392642311)
XLA Ops:
  0.0 3.2 %collective-permute-start = (bf16[128,1024]{1,0:T(8,128)(2,1)}, bf16[128,1024]{1,0:T(8,128)(2,1)S(1)}, u32[]{:S(2)}, u32[]{:S(2)}) collective-permute-start(bf16[128,1024]{1,0:T(8,128)(2,1)} %tokens_ref.1), channel_id=1, source_target_pairs={{0,1},{1,0},{2,3},{3,2},{4,5},{5,4},{6,7},{7,6},{8,9},{9,8},{10,11... | collective-permute-start | bytes 786440 | tf_op jit(solution)/shard_map/ppermute | solution.py:619
  3.2 0.7 %slice.3 = bf16[8,1024]{1,0:T(8,128)(2,1)S(1)} slice(bf16[128,1024]{1,0:T(8,128)(2,1)} %tokens_ref.1), slice={[120:128], [0:1024]} | slice | bytes 32768 | tf_op jit(solution)/shard_map/slice | solution.py:620
  3.9 1.4 %collective-permute-start.2 = (bf16[8,1024]{1,0:T(8,128)(2,1)S(1)}, bf16[8,1024]{1,0:T(8,128)(2,1)S(1)}, u32[]{:S(2)}, u32[]{:S(2)}) collective-permute-start(bf16[8,1024]{1,0:T(8,128)(2,1)S(1)} %slice.3), channel_id=1, source_target_pairs={{0,9},{1,8},{8,17},{9,16},{16,25},{17,24},{24,33},{25,32},{32,41},... | collective-permute-start | bytes 49160 | tf_op jit(solution)/shard_map/ppermute | solution.py:622
  5.3 3.2 %collective-permute-start.1 = (bf16[8,1024]{1,0:T(8,128)(2,1)S(1)}, bf16[8,1024]{1,0:T(8,128)(2,1)S(1)}, u32[]{:S(2)}, u32[]{:S(2)}) collective-permute-start(bf16[8,1024]{1,0:T(8,128)(2,1)S(1)} %slice.3), channel_id=1, source_target_pairs={{0,8},{1,9},{8,16},{9,17},{16,24},{17,25},{24,32},{25,33},{32,40},... | collective-permute-start | bytes 49160 | tf_op jit(solution)/shard_map/ppermute | solution.py:621
  8.5 2.6 %project_own.1 = (f32[128,1280]{1,0:T(8,128)S(1)}, f32[128,128]{1,0:T(8,128)S(1)}, bf16[1024,1280]{1,0:T(8,128)(2,1)S(1)}, bf16[1024,1280]{1,0:T(8,128)(2,1)S(1)}) custom-call(bf16[128,1024]{1,0:T(8,128)(2,1)} %tokens_ref.1, f32[1,2048]{1,0:T(1,128)} %bitcast.7, bf16[2048,512]{1,0:T(8,128)(2,1)} %refs_0_.1, bf16[2048,512]{1,0:T(8,128)(2,1)} %refs_1_.1, ...), custom_call_target="tpu_custom_call" | custom-call | flops 2147483648 | bytes 4194304 | tf_op jit(solution)/shard_map/project_own/pallas_call | solution.py:352
  11.2 0.0 collective-permute-done.2.halo_other_ref
  11.2 0.0 collective-permute-done.1.halo_own_ref
  11.2 0.0 collective-permute-done.other_ref
  11.2 2.8 %front.1 = (bf16[144,256]{1,0:T(8,128)(2,1)S(1)}, bf16[1024,128]{1,0:T(8,128)(2,1)S(1)}, f32[128,512]{1,0:T(8,128)S(1)}, f32[128,512]{1,0:T(8,128)S(1)}, bf16[51...) custom-call(f32[128,1280]{1,0:T(8,128)S(1)} %get-tuple-element.35.acc_ref, ...), custom_call_target="tpu_custom_call" | custom-call | flops 4294967296 | bytes 1048576 | tf_op jit(solution)/shard_map/front/pallas_call | solution.py:525
  14.0 2.8 %collective-permute-start.5 = (bf16[144,256]{1,0:T(8,128)(2,1)S(1)}, bf16[144,256]{1,0:T(8,128)(2,1)S(1)}, u32[]{:S(2)}, u32[]{:S(2)}) collective-permute-start(bf16[144,256]{1,0:T(8,128)(2,1)S(1)} %get-tuple-element.40.refs_0_), channel_id=1, source_target_pairs={{0,24},{8,0},{16,8},{24,16},{32,56},{40,32},{48,40},{56,48},{64,88... | collective-permute-start | bytes 221192 | tf_op jit(solution)/shard_map/ppermute | solution.py:629
  16.8 0.1 collective-permute-start.4
  16.9 0.7 %collective-permute-start.3 = (bf16[144,256]{1,0:T(8,128)(2,1)S(1)}, bf16[144,256]{1,0:T(8,128)(2,1)S(1)}, u32[]{:S(2)}, u32[]{:S(2)}) collective-permute-start(bf16[144,256]{1,0:T(8,128)(2,1)S(1)} %get-tuple-element.40.refs_0_), channel_id=1, source_target_pairs={{0,8},{8,16},{16,24},{24,0},{32,40},{40,48},{48,56},{56,32},{64,72... | collective-permute-start | bytes 221192 | tf_op jit(solution)/shard_map/ppermute | solution.py:629
  17.5 0.7 %collective-permute-done.5.refs_3_ = bf16[144,256]{1,0:T(8,128)(2,1)S(1)} collective-permute-done((bf16[144,256]{1,0:T(8,128)(2,1)S(1)}, bf16[144,256]{1,0:T(8,128)(2,1)S(1)}, u32[]{:S(2)}, u32[]{:S(2)}) %collective-permute-start.5) | collective-permute-done | bytes 73760 | tf_op jit(solution)/shard_map/ppermute | solution.py:629
  18.2 3.4 %collective-permute-done.4.refs_2_ = bf16[144,256]{1,0:T(8,128)(2,1)S(1)} collective-permute-done((bf16[144,256]{1,0:T(8,128)(2,1)S(1)}, bf16[144,256]{1,0:T(8,128)(2,1)S(1)}, u32[]{:S(2)}, u32[]{:S(2)}) %collective-permute-start.4) | collective-permute-done | bytes 73760 | tf_op jit(solution)/shard_map/ppermute | solution.py:629
  21.6 0.4 collective-permute-done.3.refs_1_
  22.1 0.1 assemble.1
  22.1 2.6 %collective-permute-start.14 = (bf16[528,256]{1,0:T(8,128)(2,1)S(1)}, bf16[528,256]{1,0:T(8,128)(2,1)S(1)}, u32[]{:S(2)}, u32[]{:S(2)}) collective-permute-start(bf16[528,256]{1,0:T(8,128)(2,1)S(1)} %get-tuple-element.43.block_ref), channel_id=1, source_target_pairs={{0,1},{1,0},{2,3},{3,2},{4,5},{5,4},{6,7},{7,6},{8,9},{9,8},{10,11... | collective-permute-start | bytes 811016 | tf_op jit(solution)/shard_map/ppermute | solution.py:633
  24.7 4.9 %collective-permute-start.6 = (bf16[272,256]{1,0:T(8,128)(2,1)S(1)}, bf16[272,256]{1,0:T(8,128)(2,1)S(1)}, u32[]{:S(2)}, u32[]{:S(2)}) collective-permute-start(bf16[272,256]{1,0:T(8,128)(2,1)S(1)} %get-tuple-element.41), channel_id=1, source_target_pairs={{0,32},{1,225},{8,40},{9,233},{16,48},{17,241},{24,56},{25,249},{3... | collective-permute-start | bytes 417800 | tf_op jit(solution)/shard_map/ppermute | solution.py:637
  29.6 0.7 %collective-permute-start.10 = (bf16[256,256]{1,0:T(8,128)(2,1)S(1)}, bf16[256,256]{1,0:T(8,128)(2,1)S(1)}, u32[]{:S(2)}, u32[]{:S(2)}) collective-permute-start(bf16[256,256]{1,0:T(8,128)(2,1)S(1)} %get-tuple-element.42), channel_id=1, source_target_pairs={{0,32},{1,225},{8,40},{9,233},{16,48},{17,241},{24,56},{25,249},{3... | collective-permute-start | bytes 393224 | tf_op jit(solution)/shard_map/ppermute | solution.py:637
  30.3 3.4 %collective-permute-done.10.refs_1_ = bf16[256,256]{1,0:T(8,128)(2,1)S(1)} collective-permute-done((bf16[256,256]{1,0:T(8,128)(2,1)S(1)}, bf16[256,256]{1,0:T(8,128)(2,1)S(1)}, u32[]{:S(2)}, u32[]{:S(2)}) %collective-permute-start.10) | collective-permute-done | bytes 131104 | tf_op jit(solution)/shard_map/ppermute | solution.py:637
  33.7 2.4 %collective-permute-start.11 = (bf16[256,256]{1,0:T(8,128)(2,1)S(1)}, bf16[256,256]{1,0:T(8,128)(2,1)S(1)}, u32[]{:S(2)}, u32[]{:S(2)}) collective-permute-start(bf16[256,256]{1,0:T(8,128)(2,1)S(1)} %collective-permute-done.10.refs_1_), channel_id=1, source_target_pairs={{0,32},{1,225},{8,40},{9,233},{16,48},{17,241},{24,56},{25,249},{3... | collective-permute-start | bytes 393224 | tf_op jit(solution)/shard_map/ppermute | solution.py:637
  36.1 0.0 collective-permute-done.6.refs_0_
  36.1 0.0 collective-permute-start.7
  36.1 0.0 collective-permute-done.14
  36.1 0.9 %collective-permute-start.15 = (bf16[528,256]{1,0:T(8,128)(2,1)S(1)}, bf16[528,256]{1,0:T(8,128)(2,1)S(1)}, u32[]{:S(2)}, u32[]{:S(2)}) collective-permute-start(bf16[528,256]{1,0:T(8,128)(2,1)S(1)} %collective-permute-done.14), channel_id=1, source_target_pairs={{0,32},{1,225},{8,40},{9,233},{16,48},{17,241},{24,56},{25,249},{3... | collective-permute-start | bytes 811016 | tf_op jit(solution)/shard_map/ppermute | solution.py:642
  37.0 1.2 %attend_first.1 = (f32[128,1024]{1,0:T(8,128)S(1)}, f32[8,1024]{1,0:T(8,128)S(1)}) custom-call(bf16[1024,128]{1,0:T(8,128)(2,1)S(1)} %get-tuple-element.39.wide_ref, bf16[528,256]{1,0:T(8,128)(2,1)S(1)} %get-tuple-element.43.block_ref), custom_call_target="tpu_custom_call" | custom-call | flops 4294967296 | bytes 1048576 | tf_op jit(solution)/shard_map/attend_first/pallas_call | solution.py:153
  38.1 0.0 collective-permute-done.11.refs_2_
  38.1 3.0 %collective-permute-start.12 = (bf16[256,256]{1,0:T(8,128)(2,1)S(1)}, bf16[256,256]{1,0:T(8,128)(2,1)S(1)}, u32[]{:S(2)}, u32[]{:S(2)}) collective-permute-start(bf16[256,256]{1,0:T(8,128)(2,1)S(1)} %collective-permute-done.11.refs_2_), channel_id=1, source_target_pairs={{0,32},{1,225},{8,40},{9,233},{16,48},{17,241},{24,56},{25,249},{3... | collective-permute-start | bytes 393224 | tf_op jit(solution)/shard_map/ppermute | solution.py:637
  41.1 0.0 collective-permute-done.7.refs_1_
  41.1 1.5 %collective-permute-start.8 = (bf16[272,256]{1,0:T(8,128)(2,1)S(1)}, bf16[272,256]{1,0:T(8,128)(2,1)S(1)}, u32[]{:S(2)}, u32[]{:S(2)}) collective-permute-start(bf16[272,256]{1,0:T(8,128)(2,1)S(1)} %collective-permute-done.7.refs_1_), channel_id=1, source_target_pairs={{0,32},{1,225},{8,40},{9,233},{16,48},{17,241},{24,56},{25,249},{3... | collective-permute-start | bytes 417800 | tf_op jit(solution)/shard_map/ppermute | solution.py:637
  42.6 0.6 collective-permute-done.15
  43.2 1.8 %collective-permute-start.20 = (bf16[528,256]{1,0:T(8,128)(2,1)S(1)}, bf16[528,256]{1,0:T(8,128)(2,1)S(1)}, u32[]{:S(2)}, u32[]{:S(2)}) collective-permute-start(bf16[528,256]{1,0:T(8,128)(2,1)S(1)} %collective-permute-done.15), channel_id=1, source_target_pairs={{0,1},{1,0},{2,3},{3,2},{4,5},{5,4},{6,7},{7,6},{8,9},{9,8},{10,11... | collective-permute-start | bytes 811016 | tf_op jit(solution)/shard_map/ppermute | solution.py:643
  44.9 1.0 %collective-permute-start.16 = (bf16[528,256]{1,0:T(8,128)(2,1)S(1)}, bf16[528,256]{1,0:T(8,128)(2,1)S(1)}, u32[]{:S(2)}, u32[]{:S(2)}) collective-permute-start(bf16[528,256]{1,0:T(8,128)(2,1)S(1)} %collective-permute-done.15), channel_id=1, source_target_pairs={{0,32},{1,225},{8,40},{9,233},{16,48},{17,241},{24,56},{25,249},{3... | collective-permute-start | bytes 811016 | tf_op jit(solution)/shard_map/ppermute | solution.py:642
  45.9 0.1 attend_more.4
  46.0 0.0 collective-permute-done.12.refs_2_
  46.0 1.3 %collective-permute-start.13 = (bf16[256,256]{1,0:T(8,128)(2,1)S(1)}, bf16[256,256]{1,0:T(8,128)(2,1)S(1)}, u32[]{:S(2)}, u32[]{:S(2)}) collective-permute-start(bf16[256,256]{1,0:T(8,128)(2,1)S(1)} %collective-permute-done.12.refs_2_), channel_id=1, source_target_pairs={{0,32},{1,225},{8,40},{9,233},{16,48},{17,241},{24,56},{25,249},{3... | collective-permute-start | bytes 393224 | tf_op jit(solution)/shard_map/ppermute | solution.py:637
  47.4 0.0 collective-permute-done.8.refs_1_
  47.4 1.0 %collective-permute-start.9 = (bf16[272,256]{1,0:T(8,128)(2,1)S(1)}, bf16[272,256]{1,0:T(8,128)(2,1)S(1)}, u32[]{:S(2)}, u32[]{:S(2)}) collective-permute-start(bf16[272,256]{1,0:T(8,128)(2,1)S(1)} %collective-permute-done.8.refs_1_), channel_id=1, source_target_pairs={{0,32},{1,225},{8,40},{9,233},{16,48},{17,241},{24,56},{25,249},{3... | collective-permute-start | bytes 417800 | tf_op jit(solution)/shard_map/ppermute | solution.py:637
  48.4 2.1 %collective-permute-done.16 = bf16[528,256]{1,0:T(8,128)(2,1)S(1)} collective-permute-done((bf16[528,256]{1,0:T(8,128)(2,1)S(1)}, bf16[528,256]{1,0:T(8,128)(2,1)S(1)}, u32[]{:S(2)}, u32[]{:S(2)}) %collective-permute-start.16) | collective-permute-done | bytes 270368 | tf_op jit(solution)/shard_map/ppermute | solution.py:642
  50.5 2.1 %collective-permute-start.19 = (bf16[528,256]{1,0:T(8,128)(2,1)S(1)}, bf16[528,256]{1,0:T(8,128)(2,1)S(1)}, u32[]{:S(2)}, u32[]{:S(2)}) collective-permute-start(bf16[528,256]{1,0:T(8,128)(2,1)S(1)} %collective-permute-done.16), channel_id=1, source_target_pairs={{0,1},{1,0},{2,3},{3,2},{4,5},{5,4},{6,7},{7,6},{8,9},{9,8},{10,11... | collective-permute-start | bytes 811016 | tf_op jit(solution)/shard_map/ppermute | solution.py:643
  52.6 0.0 collective-permute-start.17
  52.6 0.0 collective-permute-done.20.refs_0_
  52.6 0.1 attend_more.5
  52.7 5.5 %collective-permute-done.17 = bf16[528,256]{1,0:T(8,128)(2,1)S(1)} collective-permute-done((bf16[528,256]{1,0:T(8,128)(2,1)S(1)}, bf16[528,256]{1,0:T(8,128)(2,1)S(1)}, u32[]{:S(2)}, u32[]{:S(2)}) %collective-permute-start.17) | collective-permute-done | bytes 270368 | tf_op jit(solution)/shard_map/ppermute | solution.py:642
  58.2 2.1 %collective-permute-start.18 = (bf16[528,256]{1,0:T(8,128)(2,1)S(1)}, bf16[528,256]{1,0:T(8,128)(2,1)S(1)}, u32[]{:S(2)}, u32[]{:S(2)}) collective-permute-start(bf16[528,256]{1,0:T(8,128)(2,1)S(1)} %collective-permute-done.17), channel_id=1, source_target_pairs={{0,1},{1,0},{2,3},{3,2},{4,5},{5,4},{6,7},{7,6},{8,9},{9,8},{10,11... | collective-permute-start | bytes 811016 | tf_op jit(solution)/shard_map/ppermute | solution.py:643
  60.3 0.0 collective-permute-done.19.refs_0_
  60.3 0.1 attend_more.6
  60.4 1.1 %collective-permute-done.18.refs_0_ = bf16[528,256]{1,0:T(8,128)(2,1)S(1)} collective-permute-done((bf16[528,256]{1,0:T(8,128)(2,1)S(1)}, bf16[528,256]{1,0:T(8,128)(2,1)S(1)}, u32[]{:S(2)}, u32[]{:S(2)}) %collective-permute-start.18) | collective-permute-done | bytes 270368 | tf_op jit(solution)/shard_map/ppermute | solution.py:643
  61.5 0.0 copy-start.1
  61.5 0.0 copy-start.2
  61.5 0.1 attend_more.7
  61.6 0.0 collective-permute-done.13.two_ref
  61.6 0.0 collective-permute-done.9.one_ref
  61.6 0.5 copy-done.1
  62.1 0.0 copy-done.2
  62.1 0.0 copy-start
  62.1 1.4 %last_part.1 = (f32[64,2048]{1,0:T(8,128)S(1)}, bf16[64,2048]{1,0:T(8,128)(2,1)S(1)}) custom-call(f32[4]{0:T(128)S(1)} %copy-done.1, f32[1,128]{1,0:T(1,128)S(1)} %bitcast.6, bf16[1024,128]{1,0:T(8,128)(2,1)S(1)} %get-tuple-element.39.wide_ref, bf16[272,256]{1,0:T(8,128)(2,1)S(1)} %collective-permute-done.9.one_ref, ...), custom_call_target="tpu_custom_call" | custom-call | flops 4294967296 | bytes 4194304 | tf_op jit(solution)/shard_map/last_part/pallas_call | solution.py:238
  63.6 0.5 collective-permute-start.21
  64.0 1.2 %collective-permute-done.21.got_ref = bf16[64,2048]{1,0:T(8,128)(2,1)S(1)} collective-permute-done((bf16[64,2048]{1,0:T(8,128)(2,1)S(1)}, bf16[64,2048]{1,0:T(8,128)(2,1)S(1)}, u32[]{:S(2)}, u32[]{:S(2)}) %collective-permute-start.21) | collective-permute-done | bytes 262176 | tf_op jit(solution)/shard_map/ppermute | solution.py:658
  65.2 0.0 copy-done
  65.2 0.9 %final_norm.1 = bf16[64,2048]{1,0:T(8,128)(2,1)} custom-call(f32[64,2048]{1,0:T(8,128)S(1)} %get-tuple-element.63.keep_ref, bf16[64,2048]{1,0:T(8,128)(2,1)S(1)} %collective-permute-done.21.got_ref, f32[1,2048]{1,0:T(1,128)S(1)} %bitcast.5), custom_call_target="tpu_custom_call" | custom-call | tf_op jit(solution)/shard_map/final_norm/pallas_call | solution.py:261
Async XLA Ops:
  0.0 11.2 %collective-permute-start = (bf16[128,1024]{1,0:T(8,128)(2,1)}, bf16[128,1024]{1,0:T(8,128)(2,1)S(1)}, u32[]{:S(2)}, u32[]{:S(2)}) collective-permute-start(bf16[128,1024]{1,0:T(8,128)(2,1)} %tokens_ref.1), channel_id=1, source_target_pairs={{0,1},{1,0},{2,3},{3,2},{4,5},{5,4},{6,7},{7,6},{8,9},{9,8},{10,11... | collective-permute-start | bytes 786440 | tf_op jit(solution)/shard_map/ppermute | solution.py:619
  3.9 7.2 %collective-permute-start.2 = (bf16[8,1024]{1,0:T(8,128)(2,1)S(1)}, bf16[8,1024]{1,0:T(8,128)(2,1)S(1)}, u32[]{:S(2)}, u32[]{:S(2)}) collective-permute-start(bf16[8,1024]{1,0:T(8,128)(2,1)S(1)} %slice.3), channel_id=1, source_target_pairs={{0,9},{1,8},{8,17},{9,16},{16,25},{17,24},{24,33},{25,32},{32,41},... | collective-permute-start | bytes 49160 | tf_op jit(solution)/shard_map/ppermute | solution.py:622
  5.3 5.9 %collective-permute-start.1 = (bf16[8,1024]{1,0:T(8,128)(2,1)S(1)}, bf16[8,1024]{1,0:T(8,128)(2,1)S(1)}, u32[]{:S(2)}, u32[]{:S(2)}) collective-permute-start(bf16[8,1024]{1,0:T(8,128)(2,1)S(1)} %slice.3), channel_id=1, source_target_pairs={{0,8},{1,9},{8,16},{9,17},{16,24},{17,25},{24,32},{25,33},{32,40},... | collective-permute-start | bytes 49160 | tf_op jit(solution)/shard_map/ppermute | solution.py:621
  14.0 4.2 %collective-permute-start.5 = (bf16[144,256]{1,0:T(8,128)(2,1)S(1)}, bf16[144,256]{1,0:T(8,128)(2,1)S(1)}, u32[]{:S(2)}, u32[]{:S(2)}) collective-permute-start(bf16[144,256]{1,0:T(8,128)(2,1)S(1)} %get-tuple-element.40.refs_0_), channel_id=1, source_target_pairs={{0,24},{8,0},{16,8},{24,16},{32,56},{40,32},{48,40},{56,48},{64,88... | collective-permute-start | bytes 221192 | tf_op jit(solution)/shard_map/ppermute | solution.py:629
  16.8 4.8 %collective-permute-start.4 = (bf16[144,256]{1,0:T(8,128)(2,1)S(1)}, bf16[144,256]{1,0:T(8,128)(2,1)S(1)}, u32[]{:S(2)}, u32[]{:S(2)}) collective-permute-start(bf16[144,256]{1,0:T(8,128)(2,1)S(1)} %get-tuple-element.40.refs_0_), channel_id=1, source_target_pairs={{0,16},{8,24},{16,0},{24,8},{32,48},{40,56},{48,32},{56,40},{64,80... | collective-permute-start | bytes 221192 | tf_op jit(solution)/shard_map/ppermute | solution.py:629
  16.9 5.2 %collective-permute-start.3 = (bf16[144,256]{1,0:T(8,128)(2,1)S(1)}, bf16[144,256]{1,0:T(8,128)(2,1)S(1)}, u32[]{:S(2)}, u32[]{:S(2)}) collective-permute-start(bf16[144,256]{1,0:T(8,128)(2,1)S(1)} %get-tuple-element.40.refs_0_), channel_id=1, source_target_pairs={{0,8},{8,16},{16,24},{24,0},{32,40},{40,48},{48,56},{56,32},{64,72... | collective-permute-start | bytes 221192 | tf_op jit(solution)/shard_map/ppermute | solution.py:629
  22.1 14.0 %collective-permute-start.14 = (bf16[528,256]{1,0:T(8,128)(2,1)S(1)}, bf16[528,256]{1,0:T(8,128)(2,1)S(1)}, u32[]{:S(2)}, u32[]{:S(2)}) collective-permute-start(bf16[528,256]{1,0:T(8,128)(2,1)S(1)} %get-tuple-element.43.block_ref), channel_id=1, source_target_pairs={{0,1},{1,0},{2,3},{3,2},{4,5},{5,4},{6,7},{7,6},{8,9},{9,8},{10,11... | collective-permute-start | bytes 811016 | tf_op jit(solution)/shard_map/ppermute | solution.py:633
  24.7 11.4 %collective-permute-start.6 = (bf16[272,256]{1,0:T(8,128)(2,1)S(1)}, bf16[272,256]{1,0:T(8,128)(2,1)S(1)}, u32[]{:S(2)}, u32[]{:S(2)}) collective-permute-start(bf16[272,256]{1,0:T(8,128)(2,1)S(1)} %get-tuple-element.41), channel_id=1, source_target_pairs={{0,32},{1,225},{8,40},{9,233},{16,48},{17,241},{24,56},{25,249},{3... | collective-permute-start | bytes 417800 | tf_op jit(solution)/shard_map/ppermute | solution.py:637
  29.6 4.1 %collective-permute-start.10 = (bf16[256,256]{1,0:T(8,128)(2,1)S(1)}, bf16[256,256]{1,0:T(8,128)(2,1)S(1)}, u32[]{:S(2)}, u32[]{:S(2)}) collective-permute-start(bf16[256,256]{1,0:T(8,128)(2,1)S(1)} %get-tuple-element.42), channel_id=1, source_target_pairs={{0,32},{1,225},{8,40},{9,233},{16,48},{17,241},{24,56},{25,249},{3... | collective-permute-start | bytes 393224 | tf_op jit(solution)/shard_map/ppermute | solution.py:637
  33.7 4.5 %collective-permute-start.11 = (bf16[256,256]{1,0:T(8,128)(2,1)S(1)}, bf16[256,256]{1,0:T(8,128)(2,1)S(1)}, u32[]{:S(2)}, u32[]{:S(2)}) collective-permute-start(bf16[256,256]{1,0:T(8,128)(2,1)S(1)} %collective-permute-done.10.refs_1_), channel_id=1, source_target_pairs={{0,32},{1,225},{8,40},{9,233},{16,48},{17,241},{24,56},{25,249},{3... | collective-permute-start | bytes 393224 | tf_op jit(solution)/shard_map/ppermute | solution.py:637
  36.1 5.0 %collective-permute-start.7 = (bf16[272,256]{1,0:T(8,128)(2,1)S(1)}, bf16[272,256]{1,0:T(8,128)(2,1)S(1)}, u32[]{:S(2)}, u32[]{:S(2)}) collective-permute-start(bf16[272,256]{1,0:T(8,128)(2,1)S(1)} %collective-permute-done.6.refs_0_), channel_id=1, source_target_pairs={{0,32},{1,225},{8,40},{9,233},{16,48},{17,241},{24,56},{25,249},{3... | collective-permute-start | bytes 417800 | tf_op jit(solution)/shard_map/ppermute | solution.py:637
  36.1 7.1 %collective-permute-start.15 = (bf16[528,256]{1,0:T(8,128)(2,1)S(1)}, bf16[528,256]{1,0:T(8,128)(2,1)S(1)}, u32[]{:S(2)}, u32[]{:S(2)}) collective-permute-start(bf16[528,256]{1,0:T(8,128)(2,1)S(1)} %collective-permute-done.14), channel_id=1, source_target_pairs={{0,32},{1,225},{8,40},{9,233},{16,48},{17,241},{24,56},{25,249},{3... | collective-permute-start | bytes 811016 | tf_op jit(solution)/shard_map/ppermute | solution.py:642
  38.1 7.9 %collective-permute-start.12 = (bf16[256,256]{1,0:T(8,128)(2,1)S(1)}, bf16[256,256]{1,0:T(8,128)(2,1)S(1)}, u32[]{:S(2)}, u32[]{:S(2)}) collective-permute-start(bf16[256,256]{1,0:T(8,128)(2,1)S(1)} %collective-permute-done.11.refs_2_), channel_id=1, source_target_pairs={{0,32},{1,225},{8,40},{9,233},{16,48},{17,241},{24,56},{25,249},{3... | collective-permute-start | bytes 393224 | tf_op jit(solution)/shard_map/ppermute | solution.py:637
  41.1 6.3 %collective-permute-start.8 = (bf16[272,256]{1,0:T(8,128)(2,1)S(1)}, bf16[272,256]{1,0:T(8,128)(2,1)S(1)}, u32[]{:S(2)}, u32[]{:S(2)}) collective-permute-start(bf16[272,256]{1,0:T(8,128)(2,1)S(1)} %collective-permute-done.7.refs_1_), channel_id=1, source_target_pairs={{0,32},{1,225},{8,40},{9,233},{16,48},{17,241},{24,56},{25,249},{3... | collective-permute-start | bytes 417800 | tf_op jit(solution)/shard_map/ppermute | solution.py:637
  43.2 9.4 %collective-permute-start.20 = (bf16[528,256]{1,0:T(8,128)(2,1)S(1)}, bf16[528,256]{1,0:T(8,128)(2,1)S(1)}, u32[]{:S(2)}, u32[]{:S(2)}) collective-permute-start(bf16[528,256]{1,0:T(8,128)(2,1)S(1)} %collective-permute-done.15), channel_id=1, source_target_pairs={{0,1},{1,0},{2,3},{3,2},{4,5},{5,4},{6,7},{7,6},{8,9},{9,8},{10,11... | collective-permute-start | bytes 811016 | tf_op jit(solution)/shard_map/ppermute | solution.py:643
  44.9 5.6 %collective-permute-start.16 = (bf16[528,256]{1,0:T(8,128)(2,1)S(1)}, bf16[528,256]{1,0:T(8,128)(2,1)S(1)}, u32[]{:S(2)}, u32[]{:S(2)}) collective-permute-start(bf16[528,256]{1,0:T(8,128)(2,1)S(1)} %collective-permute-done.15), channel_id=1, source_target_pairs={{0,32},{1,225},{8,40},{9,233},{16,48},{17,241},{24,56},{25,249},{3... | collective-permute-start | bytes 811016 | tf_op jit(solution)/shard_map/ppermute | solution.py:642
  46.0 15.5 %collective-permute-start.13 = (bf16[256,256]{1,0:T(8,128)(2,1)S(1)}, bf16[256,256]{1,0:T(8,128)(2,1)S(1)}, u32[]{:S(2)}, u32[]{:S(2)}) collective-permute-start(bf16[256,256]{1,0:T(8,128)(2,1)S(1)} %collective-permute-done.12.refs_2_), channel_id=1, source_target_pairs={{0,32},{1,225},{8,40},{9,233},{16,48},{17,241},{24,56},{25,249},{3... | collective-permute-start | bytes 393224 | tf_op jit(solution)/shard_map/ppermute | solution.py:637
  47.4 14.2 %collective-permute-start.9 = (bf16[272,256]{1,0:T(8,128)(2,1)S(1)}, bf16[272,256]{1,0:T(8,128)(2,1)S(1)}, u32[]{:S(2)}, u32[]{:S(2)}) collective-permute-start(bf16[272,256]{1,0:T(8,128)(2,1)S(1)} %collective-permute-done.8.refs_1_), channel_id=1, source_target_pairs={{0,32},{1,225},{8,40},{9,233},{16,48},{17,241},{24,56},{25,249},{3... | collective-permute-start | bytes 417800 | tf_op jit(solution)/shard_map/ppermute | solution.py:637
  50.5 9.7 %collective-permute-start.19 = (bf16[528,256]{1,0:T(8,128)(2,1)S(1)}, bf16[528,256]{1,0:T(8,128)(2,1)S(1)}, u32[]{:S(2)}, u32[]{:S(2)}) collective-permute-start(bf16[528,256]{1,0:T(8,128)(2,1)S(1)} %collective-permute-done.16), channel_id=1, source_target_pairs={{0,1},{1,0},{2,3},{3,2},{4,5},{5,4},{6,7},{7,6},{8,9},{9,8},{10,11... | collective-permute-start | bytes 811016 | tf_op jit(solution)/shard_map/ppermute | solution.py:643
  52.6 5.6 %collective-permute-start.17 = (bf16[528,256]{1,0:T(8,128)(2,1)S(1)}, bf16[528,256]{1,0:T(8,128)(2,1)S(1)}, u32[]{:S(2)}, u32[]{:S(2)}) collective-permute-start(bf16[528,256]{1,0:T(8,128)(2,1)S(1)} %collective-permute-done.16), channel_id=1, source_target_pairs={{0,32},{1,225},{8,40},{9,233},{16,48},{17,241},{24,56},{25,249},{3... | collective-permute-start | bytes 811016 | tf_op jit(solution)/shard_map/ppermute | solution.py:642
  58.2 3.2 %collective-permute-start.18 = (bf16[528,256]{1,0:T(8,128)(2,1)S(1)}, bf16[528,256]{1,0:T(8,128)(2,1)S(1)}, u32[]{:S(2)}, u32[]{:S(2)}) collective-permute-start(bf16[528,256]{1,0:T(8,128)(2,1)S(1)} %collective-permute-done.17), channel_id=1, source_target_pairs={{0,1},{1,0},{2,3},{3,2},{4,5},{5,4},{6,7},{7,6},{8,9},{9,8},{10,11... | collective-permute-start | bytes 811016 | tf_op jit(solution)/shard_map/ppermute | solution.py:643
  61.5 0.7 copy-start.1
  61.5 0.7 %copy-start.2 = (f32[128]{0:T(128)S(1)}, f32[128]{0:T(128)}, u32[]{:S(2)}) copy-start(f32[128]{0:T(128)} %param.28) | copy-start | bytes 1540
  62.1 3.1 %copy-start = (f32[2048]{0:T(1024)S(1)}, f32[2048]{0:T(1024)}, u32[]{:S(2)}) copy-start(f32[2048]{0:T(1024)} %param.31) | copy-start | bytes 24580
  63.6 1.6 %collective-permute-start.21 = (bf16[64,2048]{1,0:T(8,128)(2,1)S(1)}, bf16[64,2048]{1,0:T(8,128)(2,1)S(1)}, u32[]{:S(2)}, u32[]{:S(2)}) collective-permute-start(bf16[64,2048]{1,0:T(8,128)(2,1)S(1)} %get-tuple-element.64), channel_id=1, source_target_pairs={{0,1},{1,0},{2,3},{3,2},{4,5},{5,4},{6,7},{7,6},{8,9},{9,8},{10,11... | collective-permute-start | bytes 786440 | tf_op jit(solution)/shard_map/ppermute | solution.py:658
where the time goes:
time: 66.3 us; the launch traced here: 66.1 us
  starting transfers between devices  36.9 us (56%)
  waiting for transfers between devices  18.4 us (28%)
  Pallas kernels  9.32 us (14%)
  local copies, waits for them, and re-layouts  1.28 us (2%)
    ppermute x8, starting transfers between devices, layer(): same[i] = lax.ppermute(same[i], ('sp', 'tp'), around())  14.8 us
    ppermute x3, waiting for transfers between devices, layer(): cross = lax.ppermute(cross, ('sp', 'tp'), around())  8.21 us
    ppermute x3, starting transfers between devices, layer(): other = lax.ppermute(cross, 'tp', swap)  5.89 us
    ppermute x3, waiting for transfers between devices, layer(): lax.ppermute(piece, 'sp', sp_pairs(0, r))  4.51 us
    ppermute x3, starting transfers between devices, layer(): lax.ppermute(piece, 'sp', sp_pairs(0, r))  3.56 us
    ppermute x8, waiting for transfers between devices, layer(): same[i] = lax.ppermute(same[i], ('sp', 'tp'), around())  3.4 us
    ppermute x1, starting transfers between devices, layer(): halo_own = lax.ppermute(ends, ('sp', 'tp'), later(0))  3.2 us
    ppermute x1, starting transfers between devices, layer(): other = lax.ppermute(tokens, 'tp', swap)  3.2 us
  transfers between devices with their start and end apart: 22, of which 9 were waited for; matrix products, arithmetic and copies ran while one was open for 1% of the time, Pallas kernels for 6%

commit v1 on v0

--- a/solution.py
+++ b/solution.py
@@ -34,6 +34,10 @@
         for z, y in [divmod(i, NY)]
         for t in range(2)
     ]
+
+
+def along_y(piece, distance):
+    return lax.ppermute(piece, "sp", sp_pairs(0, distance))
 
 
 def later(flip):
@@ -143,7 +147,6 @@
         take_block(step, core == up_core, parts, *refs)
 
 
-SMEM = pl.BlockSpec(memory_space=pltpu.SMEM)
 PARAMS = pltpu.CompilerParams(vmem_limit_bytes=16 << 20)
 VMEM = pl.BlockSpec(memory_space=pltpu.VMEM)
 ANY = pl.BlockSpec(memory_space=pltpu.HBM)
@@ -219,7 +222,7 @@
     for head in range(heads):
         one = slice(head * rows, (head + 1) * rows)
         two = slice((heads + head) * rows, (heads + head + 1) * rows)
-        out = acc_ref[:, one] * inverse[:, one] - lambda_ref[head] * (
+        out = acc_ref[:, one] * inverse[:, one] - lambda_ref[0:1, head : head + 1] * (
             acc_ref[:, two] * inverse[:, two]
         )
         mean = jnp.mean(out * out, axis=0, keepdims=True)
@@ -241,7 +244,7 @@
             jax.ShapeDtypeStruct((rows // 2, cols), f32),
             jax.ShapeDtypeStruct((rows // 2, cols), bf16),
         ),
-        in_specs=[SMEM] + [VMEM] * 11,
+        in_specs=[VMEM] * 12,
         out_specs=(VMEM, VMEM),
         scratch_shapes=[pltpu.VMEM(a.shape, f32) for a in state]
         + attend_scratch(2 * halves[1].shape[0]),
@@ -386,12 +389,19 @@
     extra_hbm,
     out_recur_hbm,
     out_attend_hbm,
+    lambda_hbm,
+    head_gain_hbm,
+    out_gain_hbm,
     piece_ref,
-    wide_ref,
+    scaled_ref,
+    inverse_ref,
     cum_ref,
     state_ref,
     out_recur_ref,
     out_attend_ref,
+    lambda_ref,
+    head_gain_ref,
+    out_gain_ref,
     padded_ref,
     gain_ref,
     taps_ref,
@@ -414,6 +424,9 @@
             (extra_hbm, extra_ref),
             (out_recur_hbm, out_recur_ref),
             (out_attend_hbm, out_attend_ref),
+            (lambda_hbm, lambda_ref),
+            (head_gain_hbm, head_gain_ref),
+            (out_gain_hbm, out_gain_ref),
         ],
         sems,
     )
@@ -429,6 +442,8 @@
     square = square_ref[:, 0:1] + jnp.sum(other * other, axis=1, keepdims=True)
     inverse = lax.rsqrt(square / D + norm_eps)
     scaled_other = scaled(other, theirs)
+    scaled_ref[...] = scaled_other
+    inverse_ref[...] = jnp.broadcast_to(inverse, inverse_ref.shape)
 
     def project(at, count):
         lanes = slice(at, at + count)
@@ -453,16 +468,6 @@
     at = own_w_ref.shape[1] - 2 * HEAD - DV
     piece_ref[:rows, : 2 * HEAD] = project(at, 2 * HEAD).astype(bf16)
     piece_ref[:rows, 2 * HEAD :] = project(at + 2 * HEAD, DV).astype(bf16)
-
-    queries = project(cols, at - cols).astype(bf16) * HEAD ** (-0.5)
-    heads = queries.shape[1] // (2 * HEAD)
-    first = lax.broadcasted_iota(jnp.int32, (rows, 2 * HEAD), 1) < HEAD
-    for head in range(heads):
-        part = queries[:, head * 2 * HEAD : (head + 1) * 2 * HEAD]
-        zero = jnp.zeros_like(part)
-        wide_ref[head * rows : (head + 1) * rows, :] = jnp.where(first, part, zero)
-        begin = (heads + head) * rows
-        wide_ref[begin : begin + rows, :] = jnp.where(first, zero, part)
 
     for copy in copies[1:6]:
         copy.wait()
@@ -518,28 +523,56 @@
         copy.wait()
 
 
-def front(own, other, halos, small, out_weights, cols):
+def front(own, other, halos, small, later_uses, cols):
     rows = other.shape[0]
-    queries = own[0].shape[1] - cols - 2 * HEAD - DV
     whole = jax.ShapeDtypeStruct((rows, cols), f32)
     return pl.pallas_call(
         front_kernel,
         out_shape=(
             jax.ShapeDtypeStruct((rows + EXTRA, 2 * HEAD + DV), bf16),
-            jax.ShapeDtypeStruct((2 * rows * queries // (2 * HEAD), 2 * HEAD), bf16),
+            jax.ShapeDtypeStruct(other.shape, bf16),
+            jax.ShapeDtypeStruct((rows, 128), f32),
             whole,
             whole,
-            *(jax.ShapeDtypeStruct(w.shape, bf16) for w in out_weights),
+            *(jax.ShapeDtypeStruct(w.shape, w.dtype) for w in later_uses),
         ),
-        in_specs=[VMEM] * 7 + [ANY] * 8,
-        out_specs=(VMEM,) * 6,
+        in_specs=[VMEM] * 7 + [ANY] * 11,
+        out_specs=(VMEM,) * 10,
         scratch_shapes=[pltpu.VMEM((rows + 8, cols), f32)]
         + [pltpu.VMEM(a.shape, a.dtype) for a in small]
-        + [pltpu.SemaphoreType.DMA((8,))],
+        + [pltpu.SemaphoreType.DMA((11,))],
         compiler_params=PARAMS,
         name="front",
         cost_estimate=pl.CostEstimate(flops=4 << 30, bytes_accessed=1 << 20, transcendentals=0),
-    )(*own, other, *halos, *in_hbm(*small, *out_weights))
+    )(*own, other, *halos, *in_hbm(*small, *later_uses))
+
+
+def query_kernel(acc_ref, scaled_ref, inverse_ref, w_ref, wide_ref, *, begin, count):
+    rows = scaled_ref.shape[0]
+    lanes = slice(begin, begin + count)
+    part = jnp.dot(scaled_ref[...], w_ref[:, lanes], preferred_element_type=f32)
+    queries = ((acc_ref[:, lanes] + part) * inverse_ref[:, 0:1]).astype(bf16) * HEAD ** (-0.5)
+    heads = count // (2 * HEAD)
+    first = lax.broadcasted_iota(jnp.int32, (rows, 2 * HEAD), 1) < HEAD
+    for head in range(heads):
+        part = queries[:, head * 2 * HEAD : (head + 1) * 2 * HEAD]
+        zero = jnp.zeros_like(part)
+        wide_ref[head * rows : (head + 1) * rows, :] = jnp.where(first, part, zero)
+        at = (heads + head) * rows
+        wide_ref[at : at + rows, :] = jnp.where(first, zero, part)
+
+
+def project_queries(acc, scaled, inverse, other_w, begin, count):
+    rows = scaled.shape[0]
+    return pl.pallas_call(
+        functools.partial(query_kernel, begin=begin, count=count),
+        out_shape=jax.ShapeDtypeStruct((count // HEAD * rows, 2 * HEAD), bf16),
+        in_specs=[VMEM] * 4,
+        out_specs=VMEM,
+        compiler_params=PARAMS,
+        name="project_queries",
+        cost_estimate=pl.CostEstimate(flops=1 << 30, bytes_accessed=1 << 20, transcendentals=0),
+    )(acc, scaled, inverse, other_w)
 
 
 def assemble_kernel(*refs):
@@ -622,11 +655,20 @@
     halo_other = lax.ppermute(ends, ("sp", "tp"), later(1))
     own = project_own(tokens, gain, *weights)
     small = (gain, conv_weight, w_gate_decay, w_gate_input, decay_base[None, :], extra_decay.T)
-    piece, wide, cum, local, w_out_recur, w_out_attend = front(
-        own, other, (halo_own, halo_other), small, (w_out_recur, w_out_attend), recur_cols
-    )
-
-    pieces = [piece] + [lax.ppermute(piece, "sp", sp_pairs(0, r)) for r in range(1, NY)]
+    later_uses = (
+        w_out_recur,
+        w_out_attend,
+        mix_lambda[None, :],
+        head_gain[None, :],
+        out_gain[None, :],
+    )
+    piece, scaled, inverse, cum, local, *later_uses = front(
+        own, other, (halo_own, halo_other), small, later_uses, recur_cols
+    )
+    w_out_recur, w_out_attend, lambdas, head_gain, out_gain = later_uses
+    wide = project_queries(own[0], scaled, inverse, own[3], recur_cols, w_query.shape[1])
+
+    pieces = [piece] + [along_y(piece, r) for r in range(1, NY)]
     block, *same, carry = assemble(pieces, recur_cols)
 
     state = (*attend_first(wide, block), carry)
@@ -644,8 +686,8 @@
         waiting = [((other,), step, 1)]
     state = attend_more(wide, waiting, state)
     keep, send = last_part(
-        mix_lambda,
-        head_gain[None, :],
+        lambdas,
+        head_gain,
         wide,
         same,
         NZ // 2,
@@ -656,7 +698,7 @@
         w_out_attend,
     )
     got = lax.ppermute(send, "tp", swap)
-    return final_norm(keep, got, out_gain[None, :])
+    return final_norm(keep, got, out_gain)
 
 
 def solution(mesh):

time: 66.3 us -> 65.2 us (0.983)
  transfers between devices with their start and end apart: 22 -> 22, of which waited for: 9 -> 9; matrix products, arithmetic and copies ran while one was open for 1% -> 1% of each run, Pallas kernels for 6% -> 7%
where the time goes in v1:
time: 65.2 us; the launch traced here: 64.9 us
  starting transfers between devices  37 us (57%)
  waiting for transfers between devices  18 us (28%)
  Pallas kernels  9.03 us (14%)
  local copies, waits for them, and re-layouts  0.72 us (1%)
    ppermute x8, starting transfers between devices, layer(): same[i] = lax.ppermute(same[i], ('sp', 'tp'), around())  14.9 us
    ppermute x3, waiting for transfers between devices, layer(): cross = lax.ppermute(cross, ('sp', 'tp'), around())  8.2 us
    ppermute x3, starting transfers between devices, layer(): other = lax.ppermute(cross, 'tp', swap)  5.89 us
    ppermute x3, waiting for transfers between devices, along_y(): return lax.ppermute(piece, 'sp', sp_pairs(0, distance))  4.51 us
    ppermute x3, starting transfers between devices, along_y(): return lax.ppermute(piece, 'sp', sp_pairs(0, distance))  3.56 us
    ppermute x1, starting transfers between devices, layer(): halo_own = lax.ppermute(ends, ('sp', 'tp'), later(0))  3.2 us
    ppermute x1, starting transfers between devices, layer(): other = lax.ppermute(tokens, 'tp', swap)  3.2 us
    ppermute x8, waiting for transfers between devices, layer(): same[i] = lax.ppermute(same[i], ('sp', 'tp'), around())  3.04 us
  transfers between devices with their start and end apart: 22, of which 9 were waited for; matrix products, arithmetic and copies ran while one was open for 1% of the time, Pallas kernels for 7%

profile of v1, /device:TPU:1, one launch (start us, length us, event | category | flops | bytes accessed | tf_op | source)
XLA Modules:
  0.0 64.9 jit_solution(8318315728875683219)
XLA Ops:
  0.0 3.2 %collective-permute-start = (bf16[128,1024]{1,0:T(8,128)(2,1)}, bf16[128,1024]{1,0:T(8,128)(2,1)S(1)}, u32[]{:S(2)}, u32[]{:S(2)}) collective-permute-start(bf16[128,1024]{1,0:T(8,128)(2,1)} %tokens_ref.1), channel_id=1, source_target_pairs={{0,1},{1,0},{2,3},{3,2},{4,5},{5,4},{6,7},{7,6},{8,9},{9,8},{10,11... | collective-permute-start | bytes 786440 | tf_op jit(solution)/shard_map/ppermute | solution.py:652
  3.2 0.7 %slice.3 = bf16[8,1024]{1,0:T(8,128)(2,1)S(1)} slice(bf16[128,1024]{1,0:T(8,128)(2,1)} %tokens_ref.1), slice={[120:128], [0:1024]} | slice | bytes 32768 | tf_op jit(solution)/shard_map/slice | solution.py:653
  3.9 1.4 %collective-permute-start.2 = (bf16[8,1024]{1,0:T(8,128)(2,1)S(1)}, bf16[8,1024]{1,0:T(8,128)(2,1)S(1)}, u32[]{:S(2)}, u32[]{:S(2)}) collective-permute-start(bf16[8,1024]{1,0:T(8,128)(2,1)S(1)} %slice.3), channel_id=1, source_target_pairs={{0,9},{1,8},{8,17},{9,16},{16,25},{17,24},{24,33},{25,32},{32,41},... | collective-permute-start | bytes 49160 | tf_op jit(solution)/shard_map/ppermute | solution.py:655
  5.3 3.2 %collective-permute-start.1 = (bf16[8,1024]{1,0:T(8,128)(2,1)S(1)}, bf16[8,1024]{1,0:T(8,128)(2,1)S(1)}, u32[]{:S(2)}, u32[]{:S(2)}) collective-permute-start(bf16[8,1024]{1,0:T(8,128)(2,1)S(1)} %slice.3), channel_id=1, source_target_pairs={{0,8},{1,9},{8,16},{9,17},{16,24},{17,25},{24,32},{25,33},{32,40},... | collective-permute-start | bytes 49160 | tf_op jit(solution)/shard_map/ppermute | solution.py:654
  8.5 2.6 %project_own.1 = (f32[128,1280]{1,0:T(8,128)S(1)}, f32[128,128]{1,0:T(8,128)S(1)}, bf16[1024,1280]{1,0:T(8,128)(2,1)S(1)}, bf16[1024,1280]{1,0:T(8,128)(2,1)S(1)}) custom-call(bf16[128,1024]{1,0:T(8,128)(2,1)} %tokens_ref.1, f32[1,2048]{1,0:T(1,128)} %bitcast.6, bf16[2048,512]{1,0:T(8,128)(2,1)} %refs_0_.1, bf16[2048,512]{1,0:T(8,128)(2,1)} %refs_1_.1, ...), custom_call_target="tpu_custom_call" | custom-call | flops 2147483648 | bytes 4194304 | tf_op jit(solution)/shard_map/project_own/pallas_call | solution.py:355
  11.2 0.0 collective-permute-done.2.halo_other_ref
  11.2 0.0 collective-permute-done.1.halo_own_ref
  11.2 0.0 collective-permute-done.other_ref
  11.2 2.7 %front.1 = (bf16[144,256]{1,0:T(8,128)(2,1)S(1)}, bf16[128,1024]{1,0:T(8,128)(2,1)S(1)}, f32[128,128]{1,0:T(8,128)S(1)}, f32[128,512]{1,0:T(8,128)S(1)}, f32[128...) custom-call(f32[128,1280]{1,0:T(8,128)S(1)} %get-tuple-element.39.ac, ...), custom_call_target="tpu_custom_call" | custom-call | flops 4294967296 | bytes 1048576 | tf_op jit(solution)/shard_map/front/pallas_call | solution.py:529
  13.9 2.8 %collective-permute-start.5 = (bf16[144,256]{1,0:T(8,128)(2,1)S(1)}, bf16[144,256]{1,0:T(8,128)(2,1)S(1)}, u32[]{:S(2)}, u32[]{:S(2)}) collective-permute-start(bf16[144,256]{1,0:T(8,128)(2,1)S(1)} %get-tuple-element.47.refs_0_), channel_id=1, source_target_pairs={{0,24},{8,0},{16,8},{24,16},{32,56},{40,32},{48,40},{56,48},{64,88... | collective-permute-start | bytes 221192 | tf_op jit(solution)/shard_map/ppermute | solution.py:40
  16.7 0.1 collective-permute-start.4
  16.7 0.7 %collective-permute-start.3 = (bf16[144,256]{1,0:T(8,128)(2,1)S(1)}, bf16[144,256]{1,0:T(8,128)(2,1)S(1)}, u32[]{:S(2)}, u32[]{:S(2)}) collective-permute-start(bf16[144,256]{1,0:T(8,128)(2,1)S(1)} %get-tuple-element.47.refs_0_), channel_id=1, source_target_pairs={{0,8},{8,16},{16,24},{24,0},{32,40},{40,48},{48,56},{56,32},{64,72... | collective-permute-start | bytes 221192 | tf_op jit(solution)/shard_map/ppermute | solution.py:40
  17.4 0.7 %collective-permute-done.5.refs_3_ = bf16[144,256]{1,0:T(8,128)(2,1)S(1)} collective-permute-done((bf16[144,256]{1,0:T(8,128)(2,1)S(1)}, bf16[144,256]{1,0:T(8,128)(2,1)S(1)}, u32[]{:S(2)}, u32[]{:S(2)}) %collective-permute-start.5) | collective-permute-done | bytes 73760 | tf_op jit(solution)/shard_map/ppermute | solution.py:40
  18.1 3.4 %collective-permute-done.4.refs_2_ = bf16[144,256]{1,0:T(8,128)(2,1)S(1)} collective-permute-done((bf16[144,256]{1,0:T(8,128)(2,1)S(1)}, bf16[144,256]{1,0:T(8,128)(2,1)S(1)}, u32[]{:S(2)}, u32[]{:S(2)}) %collective-permute-start.4) | collective-permute-done | bytes 73760 | tf_op jit(solution)/shard_map/ppermute | solution.py:40
  21.5 0.4 collective-permute-done.3.refs_1_
  21.9 0.1 assemble.1
  22.0 2.6 %collective-permute-start.14 = (bf16[528,256]{1,0:T(8,128)(2,1)S(1)}, bf16[528,256]{1,0:T(8,128)(2,1)S(1)}, u32[]{:S(2)}, u32[]{:S(2)}) collective-permute-start(bf16[528,256]{1,0:T(8,128)(2,1)S(1)} %get-tuple-element.50.block_ref), channel_id=1, source_target_pairs={{0,1},{1,0},{2,3},{3,2},{4,5},{5,4},{6,7},{7,6},{8,9},{9,8},{10,11... | collective-permute-start | bytes 811016 | tf_op jit(solution)/shard_map/ppermute | solution.py:675
  24.6 4.8 %collective-permute-start.6 = (bf16[272,256]{1,0:T(8,128)(2,1)S(1)}, bf16[272,256]{1,0:T(8,128)(2,1)S(1)}, u32[]{:S(2)}, u32[]{:S(2)}) collective-permute-start(bf16[272,256]{1,0:T(8,128)(2,1)S(1)} %get-tuple-element.48), channel_id=1, source_target_pairs={{0,32},{1,225},{8,40},{9,233},{16,48},{17,241},{24,56},{25,249},{3... | collective-permute-start | bytes 417800 | tf_op jit(solution)/shard_map/ppermute | solution.py:679
  29.4 0.7 %collective-permute-start.10 = (bf16[256,256]{1,0:T(8,128)(2,1)S(1)}, bf16[256,256]{1,0:T(8,128)(2,1)S(1)}, u32[]{:S(2)}, u32[]{:S(2)}) collective-permute-start(bf16[256,256]{1,0:T(8,128)(2,1)S(1)} %get-tuple-element.49), channel_id=1, source_target_pairs={{0,32},{1,225},{8,40},{9,233},{16,48},{17,241},{24,56},{25,249},{3... | collective-permute-start | bytes 393224 | tf_op jit(solution)/shard_map/ppermute | solution.py:679
  30.2 0.3 project_queries.1.wide_ref
  30.5 3.0 %collective-permute-done.10.refs_1_ = bf16[256,256]{1,0:T(8,128)(2,1)S(1)} collective-permute-done((bf16[256,256]{1,0:T(8,128)(2,1)S(1)}, bf16[256,256]{1,0:T(8,128)(2,1)S(1)}, u32[]{:S(2)}, u32[]{:S(2)}) %collective-permute-start.10) | collective-permute-done | bytes 131104 | tf_op jit(solution)/shard_map/ppermute | solution.py:679
  33.5 2.4 %collective-permute-start.11 = (bf16[256,256]{1,0:T(8,128)(2,1)S(1)}, bf16[256,256]{1,0:T(8,128)(2,1)S(1)}, u32[]{:S(2)}, u32[]{:S(2)}) collective-permute-start(bf16[256,256]{1,0:T(8,128)(2,1)S(1)} %collective-permute-done.10.refs_1_), channel_id=1, source_target_pairs={{0,32},{1,225},{8,40},{9,233},{16,48},{17,241},{24,56},{25,249},{3... | collective-permute-start | bytes 393224 | tf_op jit(solution)/shard_map/ppermute | solution.py:679
  35.9 0.0 collective-permute-done.6.refs_0_
  36.0 0.0 collective-permute-start.7
  36.0 0.0 collective-permute-done.14
  36.0 0.9 %collective-permute-start.15 = (bf16[528,256]{1,0:T(8,128)(2,1)S(1)}, bf16[528,256]{1,0:T(8,128)(2,1)S(1)}, u32[]{:S(2)}, u32[]{:S(2)}) collective-permute-start(bf16[528,256]{1,0:T(8,128)(2,1)S(1)} %collective-permute-done.14), channel_id=1, source_target_pairs={{0,32},{1,225},{8,40},{9,233},{16,48},{17,241},{24,56},{25,249},{3... | collective-permute-start | bytes 811016 | tf_op jit(solution)/shard_map/ppermute | solution.py:684
  36.8 1.1 %attend_first.1 = (f32[128,1024]{1,0:T(8,128)S(1)}, f32[8,1024]{1,0:T(8,128)S(1)}) custom-call(bf16[1024,128]{1,0:T(8,128)(2,1)S(1)} %project_queries.1.wide_ref, bf16[528,256]{1,0:T(8,128)(2,1)S(1)} %get-tuple-element.50.block_ref), custom_call_target="tpu_custom_call" | custom-call | flops 4294967296 | bytes 1048576 | tf_op jit(solution)/shard_map/attend_first/pallas_call | solution.py:156
  38.0 0.0 collective-permute-done.11.refs_2_
  38.0 3.0 %collective-permute-start.12 = (bf16[256,256]{1,0:T(8,128)(2,1)S(1)}, bf16[256,256]{1,0:T(8,128)(2,1)S(1)}, u32[]{:S(2)}, u32[]{:S(2)}) collective-permute-start(bf16[256,256]{1,0:T(8,128)(2,1)S(1)} %collective-permute-done.11.refs_2_), channel_id=1, source_target_pairs={{0,32},{1,225},{8,40},{9,233},{16,48},{17,241},{24,56},{25,249},{3... | collective-permute-start | bytes 393224 | tf_op jit(solution)/shard_map/ppermute | solution.py:679
  41.0 0.0 collective-permute-done.7.refs_1_
  41.0 1.5 %collective-permute-start.8 = (bf16[272,256]{1,0:T(8,128)(2,1)S(1)}, bf16[272,256]{1,0:T(8,128)(2,1)S(1)}, u32[]{:S(2)}, u32[]{:S(2)}) collective-permute-start(bf16[272,256]{1,0:T(8,128)(2,1)S(1)} %collective-permute-done.7.refs_1_), channel_id=1, source_target_pairs={{0,32},{1,225},{8,40},{9,233},{16,48},{17,241},{24,56},{25,249},{3... | collective-permute-start | bytes 417800 | tf_op jit(solution)/shard_map/ppermute | solution.py:679
  42.5 0.6 collective-permute-done.15
  43.1 1.8 %collective-permute-start.20 = (bf16[528,256]{1,0:T(8,128)(2,1)S(1)}, bf16[528,256]{1,0:T(8,128)(2,1)S(1)}, u32[]{:S(2)}, u32[]{:S(2)}) collective-permute-start(bf16[528,256]{1,0:T(8,128)(2,1)S(1)} %collective-permute-done.15), channel_id=1, source_target_pairs={{0,1},{1,0},{2,3},{3,2},{4,5},{5,4},{6,7},{7,6},{8,9},{9,8},{10,11... | collective-permute-start | bytes 811016 | tf_op jit(solution)/shard_map/ppermute | solution.py:685
  44.8 1.0 %collective-permute-start.16 = (bf16[528,256]{1,0:T(8,128)(2,1)S(1)}, bf16[528,256]{1,0:T(8,128)(2,1)S(1)}, u32[]{:S(2)}, u32[]{:S(2)}) collective-permute-start(bf16[528,256]{1,0:T(8,128)(2,1)S(1)} %collective-permute-done.15), channel_id=1, source_target_pairs={{0,32},{1,225},{8,40},{9,233},{16,48},{17,241},{24,56},{25,249},{3... | collective-permute-start | bytes 811016 | tf_op jit(solution)/shard_map/ppermute | solution.py:684
  45.8 0.1 attend_more.4
  45.9 0.0 collective-permute-done.12.refs_2_
  45.9 1.4 %collective-permute-start.13 = (bf16[256,256]{1,0:T(8,128)(2,1)S(1)}, bf16[256,256]{1,0:T(8,128)(2,1)S(1)}, u32[]{:S(2)}, u32[]{:S(2)}) collective-permute-start(bf16[256,256]{1,0:T(8,128)(2,1)S(1)} %collective-permute-done.12.refs_2_), channel_id=1, source_target_pairs={{0,32},{1,225},{8,40},{9,233},{16,48},{17,241},{24,56},{25,249},{3... | collective-permute-start | bytes 393224 | tf_op jit(solution)/shard_map/ppermute | solution.py:679
  47.3 0.0 collective-permute-done.8.refs_1_
  47.3 1.0 %collective-permute-start.9 = (bf16[272,256]{1,0:T(8,128)(2,1)S(1)}, bf16[272,256]{1,0:T(8,128)(2,1)S(1)}, u32[]{:S(2)}, u32[]{:S(2)}) collective-permute-start(bf16[272,256]{1,0:T(8,128)(2,1)S(1)} %collective-permute-done.8.refs_1_), channel_id=1, source_target_pairs={{0,32},{1,225},{8,40},{9,233},{16,48},{17,241},{24,56},{25,249},{3... | collective-permute-start | bytes 417800 | tf_op jit(solution)/shard_map/ppermute | solution.py:679
  48.3 2.1 %collective-permute-done.16 = bf16[528,256]{1,0:T(8,128)(2,1)S(1)} collective-permute-done((bf16[528,256]{1,0:T(8,128)(2,1)S(1)}, bf16[528,256]{1,0:T(8,128)(2,1)S(1)}, u32[]{:S(2)}, u32[]{:S(2)}) %collective-permute-start.16) | collective-permute-done | bytes 270368 | tf_op jit(solution)/shard_map/ppermute | solution.py:684
  50.4 2.1 %collective-permute-start.19 = (bf16[528,256]{1,0:T(8,128)(2,1)S(1)}, bf16[528,256]{1,0:T(8,128)(2,1)S(1)}, u32[]{:S(2)}, u32[]{:S(2)}) collective-permute-start(bf16[528,256]{1,0:T(8,128)(2,1)S(1)} %collective-permute-done.16), channel_id=1, source_target_pairs={{0,1},{1,0},{2,3},{3,2},{4,5},{5,4},{6,7},{7,6},{8,9},{9,8},{10,11... | collective-permute-start | bytes 811016 | tf_op jit(solution)/shard_map/ppermute | solution.py:685
  52.5 0.0 collective-permute-start.17
  52.5 0.0 collective-permute-done.20.refs_0_
  52.5 0.1 attend_more.5
  52.6 5.5 %collective-permute-done.17 = bf16[528,256]{1,0:T(8,128)(2,1)S(1)} collective-permute-done((bf16[528,256]{1,0:T(8,128)(2,1)S(1)}, bf16[528,256]{1,0:T(8,128)(2,1)S(1)}, u32[]{:S(2)}, u32[]{:S(2)}) %collective-permute-start.17) | collective-permute-done | bytes 270368 | tf_op jit(solution)/shard_map/ppermute | solution.py:684
  58.1 2.1 %collective-permute-start.18 = (bf16[528,256]{1,0:T(8,128)(2,1)S(1)}, bf16[528,256]{1,0:T(8,128)(2,1)S(1)}, u32[]{:S(2)}, u32[]{:S(2)}) collective-permute-start(bf16[528,256]{1,0:T(8,128)(2,1)S(1)} %collective-permute-done.17), channel_id=1, source_target_pairs={{0,1},{1,0},{2,3},{3,2},{4,5},{5,4},{6,7},{7,6},{8,9},{9,8},{10,11... | collective-permute-start | bytes 811016 | tf_op jit(solution)/shard_map/ppermute | solution.py:685
  60.2 0.0 collective-permute-done.19.refs_0_
  60.2 0.1 attend_more.6
  60.3 1.1 %collective-permute-done.18.refs_0_ = bf16[528,256]{1,0:T(8,128)(2,1)S(1)} collective-permute-done((bf16[528,256]{1,0:T(8,128)(2,1)S(1)}, bf16[528,256]{1,0:T(8,128)(2,1)S(1)}, u32[]{:S(2)}, u32[]{:S(2)}) %collective-permute-start.18) | collective-permute-done | bytes 270368 | tf_op jit(solution)/shard_map/ppermute | solution.py:685
  61.3 0.1 attend_more.7
  61.4 0.0 collective-permute-done.13.two_ref
  61.4 0.0 collective-permute-done.9.one_ref
  61.4 0.9 %last_part.1 = (f32[64,2048]{1,0:T(8,128)S(1)}, bf16[64,2048]{1,0:T(8,128)(2,1)S(1)}) custom-call(f32[1,4]{1,0:T(1,128)S(1)} %get-tuple-element.43.lambda_ref, f32[1,128]{1,0:T(1,128)S(1)} %get-tuple-element.44.gain_ref, bf16[1024,128]{1,0:T(8,128)(2,1)S(1)} %project_queries.1.wide_ref, bf16[272,256]{1,0:T(8,128)(2,1)S(1)} %collective-permute-done.9.one_ref, ...), custom_call_target="tpu_custom_call" | custom-call | flops 4294967296 | bytes 4194304 | tf_op jit(solution)/shard_map/last_part/pallas_call | solution.py:241
  62.4 0.5 collective-permute-start.21
  62.8 1.2 %collective-permute-done.21.got_ref = bf16[64,2048]{1,0:T(8,128)(2,1)S(1)} collective-permute-done((bf16[64,2048]{1,0:T(8,128)(2,1)S(1)}, bf16[64,2048]{1,0:T(8,128)(2,1)S(1)}, u32[]{:S(2)}, u32[]{:S(2)}) %collective-permute-start.21) | collective-permute-done | bytes 262176 | tf_op jit(solution)/shard_map/ppermute | solution.py:700
  64.0 0.9 %final_norm.1 = bf16[64,2048]{1,0:T(8,128)(2,1)} custom-call(f32[64,2048]{1,0:T(8,128)S(1)} %get-tuple-element.70.keep_ref, bf16[64,2048]{1,0:T(8,128)(2,1)S(1)} %collective-permute-done.21.got_ref, f32[1,2048]{1,0:T(1,128)S(1)} %get-tuple-element.72.gain_ref), custom_call_target="tpu_custom_call" | custom-call | tf_op jit(solution)/shard_map/final_norm/pallas_call | solution.py:264
Async XLA Ops:
  0.0 11.2 %collective-permute-start = (bf16[128,1024]{1,0:T(8,128)(2,1)}, bf16[128,1024]{1,0:T(8,128)(2,1)S(1)}, u32[]{:S(2)}, u32[]{:S(2)}) collective-permute-start(bf16[128,1024]{1,0:T(8,128)(2,1)} %tokens_ref.1), channel_id=1, source_target_pairs={{0,1},{1,0},{2,3},{3,2},{4,5},{5,4},{6,7},{7,6},{8,9},{9,8},{10,11... | collective-permute-start | bytes 786440 | tf_op jit(solution)/shard_map/ppermute | solution.py:652
  3.9 7.2 %collective-permute-start.2 = (bf16[8,1024]{1,0:T(8,128)(2,1)S(1)}, bf16[8,1024]{1,0:T(8,128)(2,1)S(1)}, u32[]{:S(2)}, u32[]{:S(2)}) collective-permute-start(bf16[8,1024]{1,0:T(8,128)(2,1)S(1)} %slice.3), channel_id=1, source_target_pairs={{0,9},{1,8},{8,17},{9,16},{16,25},{17,24},{24,33},{25,32},{32,41},... | collective-permute-start | bytes 49160 | tf_op jit(solution)/shard_map/ppermute | solution.py:655
  5.3 5.9 %collective-permute-start.1 = (bf16[8,1024]{1,0:T(8,128)(2,1)S(1)}, bf16[8,1024]{1,0:T(8,128)(2,1)S(1)}, u32[]{:S(2)}, u32[]{:S(2)}) collective-permute-start(bf16[8,1024]{1,0:T(8,128)(2,1)S(1)} %slice.3), channel_id=1, source_target_pairs={{0,8},{1,9},{8,16},{9,17},{16,24},{17,25},{24,32},{25,33},{32,40},... | collective-permute-start | bytes 49160 | tf_op jit(solution)/shard_map/ppermute | solution.py:654
  13.9 4.2 %collective-permute-start.5 = (bf16[144,256]{1,0:T(8,128)(2,1)S(1)}, bf16[144,256]{1,0:T(8,128)(2,1)S(1)}, u32[]{:S(2)}, u32[]{:S(2)}) collective-permute-start(bf16[144,256]{1,0:T(8,128)(2,1)S(1)} %get-tuple-element.47.refs_0_), channel_id=1, source_target_pairs={{0,24},{8,0},{16,8},{24,16},{32,56},{40,32},{48,40},{56,48},{64,88... | collective-permute-start | bytes 221192 | tf_op jit(solution)/shard_map/ppermute | solution.py:40
  16.7 4.8 %collective-permute-start.4 = (bf16[144,256]{1,0:T(8,128)(2,1)S(1)}, bf16[144,256]{1,0:T(8,128)(2,1)S(1)}, u32[]{:S(2)}, u32[]{:S(2)}) collective-permute-start(bf16[144,256]{1,0:T(8,128)(2,1)S(1)} %get-tuple-element.47.refs_0_), channel_id=1, source_target_pairs={{0,16},{8,24},{16,0},{24,8},{32,48},{40,56},{48,32},{56,40},{64,80... | collective-permute-start | bytes 221192 | tf_op jit(solution)/shard_map/ppermute | solution.py:40
  16.7 5.2 %collective-permute-start.3 = (bf16[144,256]{1,0:T(8,128)(2,1)S(1)}, bf16[144,256]{1,0:T(8,128)(2,1)S(1)}, u32[]{:S(2)}, u32[]{:S(2)}) collective-permute-start(bf16[144,256]{1,0:T(8,128)(2,1)S(1)} %get-tuple-element.47.refs_0_), channel_id=1, source_target_pairs={{0,8},{8,16},{16,24},{24,0},{32,40},{40,48},{48,56},{56,32},{64,72... | collective-permute-start | bytes 221192 | tf_op jit(solution)/shard_map/ppermute | solution.py:40
  22.0 14.0 %collective-permute-start.14 = (bf16[528,256]{1,0:T(8,128)(2,1)S(1)}, bf16[528,256]{1,0:T(8,128)(2,1)S(1)}, u32[]{:S(2)}, u32[]{:S(2)}) collective-permute-start(bf16[528,256]{1,0:T(8,128)(2,1)S(1)} %get-tuple-element.50.block_ref), channel_id=1, source_target_pairs={{0,1},{1,0},{2,3},{3,2},{4,5},{5,4},{6,7},{7,6},{8,9},{9,8},{10,11... | collective-permute-start | bytes 811016 | tf_op jit(solution)/shard_map/ppermute | solution.py:675
  24.6 11.4 %collective-permute-start.6 = (bf16[272,256]{1,0:T(8,128)(2,1)S(1)}, bf16[272,256]{1,0:T(8,128)(2,1)S(1)}, u32[]{:S(2)}, u32[]{:S(2)}) collective-permute-start(bf16[272,256]{1,0:T(8,128)(2,1)S(1)} %get-tuple-element.48), channel_id=1, source_target_pairs={{0,32},{1,225},{8,40},{9,233},{16,48},{17,241},{24,56},{25,249},{3... | collective-permute-start | bytes 417800 | tf_op jit(solution)/shard_map/ppermute | solution.py:679
  29.4 4.1 %collective-permute-start.10 = (bf16[256,256]{1,0:T(8,128)(2,1)S(1)}, bf16[256,256]{1,0:T(8,128)(2,1)S(1)}, u32[]{:S(2)}, u32[]{:S(2)}) collective-permute-start(bf16[256,256]{1,0:T(8,128)(2,1)S(1)} %get-tuple-element.49), channel_id=1, source_target_pairs={{0,32},{1,225},{8,40},{9,233},{16,48},{17,241},{24,56},{25,249},{3... | collective-permute-start | bytes 393224 | tf_op jit(solution)/shard_map/ppermute | solution.py:679
  33.5 4.4 %collective-permute-start.11 = (bf16[256,256]{1,0:T(8,128)(2,1)S(1)}, bf16[256,256]{1,0:T(8,128)(2,1)S(1)}, u32[]{:S(2)}, u32[]{:S(2)}) collective-permute-start(bf16[256,256]{1,0:T(8,128)(2,1)S(1)} %collective-permute-done.10.refs_1_), channel_id=1, source_target_pairs={{0,32},{1,225},{8,40},{9,233},{16,48},{17,241},{24,56},{25,249},{3... | collective-permute-start | bytes 393224 | tf_op jit(solution)/shard_map/ppermute | solution.py:679
  36.0 5.0 %collective-permute-start.7 = (bf16[272,256]{1,0:T(8,128)(2,1)S(1)}, bf16[272,256]{1,0:T(8,128)(2,1)S(1)}, u32[]{:S(2)}, u32[]{:S(2)}) collective-permute-start(bf16[272,256]{1,0:T(8,128)(2,1)S(1)} %collective-permute-done.6.refs_0_), channel_id=1, source_target_pairs={{0,32},{1,225},{8,40},{9,233},{16,48},{17,241},{24,56},{25,249},{3... | collective-permute-start | bytes 417800 | tf_op jit(solution)/shard_map/ppermute | solution.py:679
  36.0 7.1 %collective-permute-start.15 = (bf16[528,256]{1,0:T(8,128)(2,1)S(1)}, bf16[528,256]{1,0:T(8,128)(2,1)S(1)}, u32[]{:S(2)}, u32[]{:S(2)}) collective-permute-start(bf16[528,256]{1,0:T(8,128)(2,1)S(1)} %collective-permute-done.14), channel_id=1, source_target_pairs={{0,32},{1,225},{8,40},{9,233},{16,48},{17,241},{24,56},{25,249},{3... | collective-permute-start | bytes 811016 | tf_op jit(solution)/shard_map/ppermute | solution.py:684
  38.0 7.9 %collective-permute-start.12 = (bf16[256,256]{1,0:T(8,128)(2,1)S(1)}, bf16[256,256]{1,0:T(8,128)(2,1)S(1)}, u32[]{:S(2)}, u32[]{:S(2)}) collective-permute-start(bf16[256,256]{1,0:T(8,128)(2,1)S(1)} %collective-permute-done.11.refs_2_), channel_id=1, source_target_pairs={{0,32},{1,225},{8,40},{9,233},{16,48},{17,241},{24,56},{25,249},{3... | collective-permute-start | bytes 393224 | tf_op jit(solution)/shard_map/ppermute | solution.py:679
  41.0 6.3 %collective-permute-start.8 = (bf16[272,256]{1,0:T(8,128)(2,1)S(1)}, bf16[272,256]{1,0:T(8,128)(2,1)S(1)}, u32[]{:S(2)}, u32[]{:S(2)}) collective-permute-start(bf16[272,256]{1,0:T(8,128)(2,1)S(1)} %collective-permute-done.7.refs_1_), channel_id=1, source_target_pairs={{0,32},{1,225},{8,40},{9,233},{16,48},{17,241},{24,56},{25,249},{3... | collective-permute-start | bytes 417800 | tf_op jit(solution)/shard_map/ppermute | solution.py:679
  43.1 9.4 %collective-permute-start.20 = (bf16[528,256]{1,0:T(8,128)(2,1)S(1)}, bf16[528,256]{1,0:T(8,128)(2,1)S(1)}, u32[]{:S(2)}, u32[]{:S(2)}) collective-permute-start(bf16[528,256]{1,0:T(8,128)(2,1)S(1)} %collective-permute-done.15), channel_id=1, source_target_pairs={{0,1},{1,0},{2,3},{3,2},{4,5},{5,4},{6,7},{7,6},{8,9},{9,8},{10,11... | collective-permute-start | bytes 811016 | tf_op jit(solution)/shard_map/ppermute | solution.py:685
  44.8 5.6 %collective-permute-start.16 = (bf16[528,256]{1,0:T(8,128)(2,1)S(1)}, bf16[528,256]{1,0:T(8,128)(2,1)S(1)}, u32[]{:S(2)}, u32[]{:S(2)}) collective-permute-start(bf16[528,256]{1,0:T(8,128)(2,1)S(1)} %collective-permute-done.15), channel_id=1, source_target_pairs={{0,32},{1,225},{8,40},{9,233},{16,48},{17,241},{24,56},{25,249},{3... | collective-permute-start | bytes 811016 | tf_op jit(solution)/shard_map/ppermute | solution.py:684
  45.9 15.5 %collective-permute-start.13 = (bf16[256,256]{1,0:T(8,128)(2,1)S(1)}, bf16[256,256]{1,0:T(8,128)(2,1)S(1)}, u32[]{:S(2)}, u32[]{:S(2)}) collective-permute-start(bf16[256,256]{1,0:T(8,128)(2,1)S(1)} %collective-permute-done.12.refs_2_), channel_id=1, source_target_pairs={{0,32},{1,225},{8,40},{9,233},{16,48},{17,241},{24,56},{25,249},{3... | collective-permute-start | bytes 393224 | tf_op jit(solution)/shard_map/ppermute | solution.py:679
  47.3 14.1 %collective-permute-start.9 = (bf16[272,256]{1,0:T(8,128)(2,1)S(1)}, bf16[272,256]{1,0:T(8,128)(2,1)S(1)}, u32[]{:S(2)}, u32[]{:S(2)}) collective-permute-start(bf16[272,256]{1,0:T(8,128)(2,1)S(1)} %collective-permute-done.8.refs_1_), channel_id=1, source_target_pairs={{0,32},{1,225},{8,40},{9,233},{16,48},{17,241},{24,56},{25,249},{3... | collective-permute-start | bytes 417800 | tf_op jit(solution)/shard_map/ppermute | solution.py:679
  50.4 9.7 %collective-permute-start.19 = (bf16[528,256]{1,0:T(8,128)(2,1)S(1)}, bf16[528,256]{1,0:T(8,128)(2,1)S(1)}, u32[]{:S(2)}, u32[]{:S(2)}) collective-permute-start(bf16[528,256]{1,0:T(8,128)(2,1)S(1)} %collective-permute-done.16), channel_id=1, source_target_pairs={{0,1},{1,0},{2,3},{3,2},{4,5},{5,4},{6,7},{7,6},{8,9},{9,8},{10,11... | collective-permute-start | bytes 811016 | tf_op jit(solution)/shard_map/ppermute | solution.py:685
  52.5 5.6 %collective-permute-start.17 = (bf16[528,256]{1,0:T(8,128)(2,1)S(1)}, bf16[528,256]{1,0:T(8,128)(2,1)S(1)}, u32[]{:S(2)}, u32[]{:S(2)}) collective-permute-start(bf16[528,256]{1,0:T(8,128)(2,1)S(1)} %collective-permute-done.16), channel_id=1, source_target_pairs={{0,32},{1,225},{8,40},{9,233},{16,48},{17,241},{24,56},{25,249},{3... | collective-permute-start | bytes 811016 | tf_op jit(solution)/shard_map/ppermute | solution.py:684
  58.1 3.2 %collective-permute-start.18 = (bf16[528,256]{1,0:T(8,128)(2,1)S(1)}, bf16[528,256]{1,0:T(8,128)(2,1)S(1)}, u32[]{:S(2)}, u32[]{:S(2)}) collective-permute-start(bf16[528,256]{1,0:T(8,128)(2,1)S(1)} %collective-permute-done.17), channel_id=1, source_target_pairs={{0,1},{1,0},{2,3},{3,2},{4,5},{5,4},{6,7},{7,6},{8,9},{9,8},{10,11... | collective-permute-start | bytes 811016 | tf_op jit(solution)/shard_map/ppermute | solution.py:685
  62.4 1.6 %collective-permute-start.21 = (bf16[64,2048]{1,0:T(8,128)(2,1)S(1)}, bf16[64,2048]{1,0:T(8,128)(2,1)S(1)}, u32[]{:S(2)}, u32[]{:S(2)}) collective-permute-start(bf16[64,2048]{1,0:T(8,128)(2,1)S(1)} %get-tuple-element.71), channel_id=1, source_target_pairs={{0,1},{1,0},{2,3},{3,2},{4,5},{5,4},{6,7},{7,6},{8,9},{9,8},{10,11... | collective-permute-start | bytes 786440 | tf_op jit(solution)/shard_map/ppermute | solution.py:700
